TPU v7x, 32 devices: a whole 2x2x4 slice. The times are simulated.
32 devices in a mesh: sp: 4 (over z), fs: 4 (over y, x), tp: 2 (over core).
Axes of the slice: x: 2, y: 2, z: 4, core: 2. Of those that a mesh axis runs over, the one named last changes fastest.
Arguments:
- tokens: bfloat16 [4, 512, 4096], P('fs', 'sp', 'tp'), may hold values from -6 to 6
- norm_gain: float32 [4096], replicated, may hold values from 0.1 to 1.9
- w_state_in: bfloat16 [4096, 2048], P(('sp', 'fs'), 'tp'), may hold values from -0.09375 to 0.09375
- w_query: bfloat16 [4096, 2048], P(('sp', 'fs'), 'tp'), may hold values from -0.3125 to 0.3125
- w_key: bfloat16 [4096, 2048], P(('sp', 'fs'), 'tp'), may hold values from -0.3125 to 0.3125
- w_value: bfloat16 [4096, 2048], P(('sp', 'fs'), 'tp'), may hold values from -0.09375 to 0.09375
- decay_re: float32 [128, 64], P('tp'), may hold values from -0.034 to -9.765625e-05
- decay_im: float32 [128, 64], P('tp'), may hold values from -3.140625 to 3.140625
- log_step: float32 [128], P('tp'), may hold values from -3.5 to -1.5
- decay_shift: float32 [4, 128, 512], P('fs', 'tp', 'sp'), may hold values from -2 to 0
- in_re: float32 [128, 64, 16], P('tp'), may hold values from -2 to 2
- in_im: float32 [128, 64, 16], P('tp'), may hold values from -2 to 2
- output_real: float32 [128, 16, 64], P('tp'), may hold values from -0.75 to 0.75
- output_imaginary: float32 [128, 16, 64], P('tp'), may hold values from -0.75 to 0.75
- skip: float32 [2048], P('tp'), may hold values from -1.2 to 1.2
- mix_weight: float32 [8], P('tp'), may hold values from 0.3 to 0.8
- head_gain: float32 [256], replicated, may hold values from 0.1 to 1.9
- w_out_state: bfloat16 [2048, 4096], P('tp'), may hold values from -0.125 to 0.125
- w_out_attn: bfloat16 [2048, 4096], P('tp'), may hold values from -0.125 to 0.125
Outputs:
- mixed: bfloat16 [4, 512, 4096], P('fs', ('sp', 'tp'))
- log_totals: float32 [4, 8, 2, 512], P('fs', 'tp', None, 'sp')
All inputs are finite; a program needn't handle non-finite values.
Results may differ from a plain program's by a relative error of at most 0.015.
Values may be sent and summed in bfloat16 or wider, within the bound.
A program may use at most 128 MiB of HBM per device.

v0:
```python
import functools
import math

import jax
import jax.numpy as jnp
from jax import lax
from jax.experimental import pallas as pl
from jax.experimental.pallas import tpu as pltpu
from jax.sharding import PartitionSpec as P


def prefix(x, axis, combine, identity):
    size, here = (lax.axis_size(axis), lax.axis_index(axis))
    everything = jax.tree.map(lambda part: lax.all_gather(part, axis), x)
    start = jax.tree.map(
        lambda part, zero: jnp.broadcast_to(jnp.asarray(zero, part.dtype), part.shape), x, identity
    )

    def hop(k, before):
        reached = k < here
        new = combine(before, jax.tree.map(lambda part: part[k], everything))
        return jax.tree.map(lambda a, b: jnp.where(reached, a, b), new, before)

    return lax.fori_loop(0, size, hop, start)


def compose(earlier, later):
    early_scale_re, early_scale_im, early_shift_re, early_shift_im = earlier
    late_scale_re, late_scale_im, late_shift_re, late_shift_im = later
    scale_re = late_scale_re * early_scale_re - late_scale_im * early_scale_im
    scale_im = late_scale_re * early_scale_im + late_scale_im * early_scale_re
    shift_re = late_scale_re * early_shift_re - late_scale_im * early_shift_im + late_shift_re
    shift_im = late_scale_re * early_shift_im + late_scale_im * early_shift_re + late_shift_im
    return (scale_re, scale_im, shift_re, shift_im)


def state_branch(
    state_in,
    decay_re,
    decay_im,
    log_step,
    decay_shift,
    in_re,
    in_im,
    output_real,
    output_imaginary,
    skip,
):
    upper_limit = lax.Precision.HIGHEST
    tok_rows = state_in.shape[0]
    group_count, state_size = decay_re.shape
    group_width = in_re.shape[2]
    flat_width = group_count * state_size
    step_size = jnp.exp(log_step)[:, None]
    numer_re = jnp.expm1(decay_re) * jnp.cos(decay_im) - 2.0 * jnp.sin(0.5 * decay_im) ** 2
    numer_im = jnp.exp(decay_re) * jnp.sin(decay_im)
    modulus = decay_re * decay_re + decay_im * decay_im
    coef_re = step_size * (numer_re * decay_re + numer_im * decay_im) / modulus
    coef_im = step_size * (numer_im * decay_re - numer_re * decay_im) / modulus
    matrix_re = coef_re[..., None] * in_re - coef_im[..., None] * in_im
    matrix_im = coef_re[..., None] * in_im + coef_im[..., None] * in_re
    inputs = state_in.astype(jnp.float32).reshape(tok_rows, group_count, group_width)
    flat_shape = (tok_rows, flat_width)
    drive_re = jnp.einsum("gpc,tgc->tgp", matrix_re, inputs, precision=upper_limit).reshape(
        flat_shape
    )
    drive_im = jnp.einsum("gpc,tgc->tgp", matrix_im, inputs, precision=upper_limit).reshape(
        flat_shape
    )
    magnitude = jnp.exp(decay_re[None] + decay_shift[0].T[:, :, None])
    factor_re = (magnitude * jnp.cos(decay_im)[None]).reshape(flat_shape)
    factor_im = (magnitude * jnp.sin(decay_im)[None]).reshape(flat_shape)
    span = math.gcd(tok_rows, 16)
    block_count = tok_rows // span

    def to_blocks(values):
        return values.reshape(block_count, span, flat_width).transpose(1, 0, 2)

    rows_in = tuple((to_blocks(values) for values in (factor_re, factor_im, drive_re, drive_im)))
    ones_blocks = jnp.ones((block_count, flat_width), jnp.float32)
    zero_blocks = jnp.zeros((block_count, flat_width), jnp.float32)

    def row_step(carry, row):
        joined = compose(carry, row)
        return (joined, joined)

    block_totals, local = lax.scan(
        row_step, (ones_blocks, zero_blocks, zero_blocks, zero_blocks), rows_in
    )
    ones_row = jnp.ones((flat_width,), jnp.float32)
    zero_row = jnp.zeros((flat_width,), jnp.float32)

    def block_step(carry, row):
        return (compose(carry, row), carry)

    totals, before = lax.scan(block_step, (ones_row, zero_row, zero_row, zero_row), block_totals)
    carried = prefix(totals, "sp", compose, (ones_row, zero_row, zero_row, zero_row))
    start_re, start_im = (carried[2], carried[3])
    enter_re = before[0] * start_re[None] - before[1] * start_im[None] + before[2]
    enter_im = before[0] * start_im[None] + before[1] * start_re[None] + before[3]
    state_real = local[2] + local[0] * enter_re[None] - local[1] * enter_im[None]
    state_imaginary = local[3] + local[0] * enter_im[None] + local[1] * enter_re[None]
    group_layout_shape = (tok_rows, group_count, state_size)
    state_real = state_real.transpose(1, 0, 2).reshape(group_layout_shape)
    state_imaginary = state_imaginary.transpose(1, 0, 2).reshape(group_layout_shape)
    result = (
        jnp.einsum("hsv,jhv->jhs", output_real, state_real, precision=upper_limit)
        - jnp.einsum("hsv,jhv->jhs", output_imaginary, state_imaginary, precision=upper_limit)
        + skip.reshape(group_count, group_width)[None] * inputs
    )
    return result.reshape(tok_rows, group_count * group_width).astype(jnp.bfloat16)


def attention_branch(queries, keys_local, values_local, mix_weight, head_gain):
    tok_rows = queries.shape[0]
    head_count = mix_weight.shape[0]
    head_dim = queries.shape[1] // (2 * head_count)
    value_dim = values_local.shape[1] // head_count
    scale = head_dim ** (-0.5)
    first_pos = lax.axis_index("sp") * tok_rows
    query_pos = first_pos + jnp.arange(tok_rows, dtype=jnp.int32)
    query_heads = queries.reshape(tok_rows, head_count, 2, head_dim)
    initial = (
        jnp.full((head_count, 2, tok_rows), -1e30, jnp.float32),
        jnp.zeros((head_count, 2, tok_rows), jnp.float32),
        jnp.zeros((head_count, 2, tok_rows, value_dim), jnp.float32),
    )
    key_piece = lax.all_gather(keys_local, "sp", axis=0, tiled=True)
    value_piece = lax.all_gather(values_local, "sp", axis=0, tiled=True)
    count = key_piece.shape[0]
    block = math.gcd(count, 512)

    def one_block(index, inner):
        run_max, run_total, run_accum = inner
        offset = index * block
        key_block = lax.dynamic_slice_in_dim(key_piece, offset, block, 0).reshape(
            block, head_count, 2, head_dim
        )
        value_block = lax.dynamic_slice_in_dim(value_piece, offset, block, 0).reshape(
            block, head_count, value_dim
        )
        key_pos = offset + jnp.arange(block, dtype=jnp.int32)
        scores = (
            jnp.einsum(
                "qhmd,khmd->hmqk", query_heads, key_block, preferred_element_type=jnp.float32
            )
            * scale
        )
        allowed = key_pos[None, :] <= query_pos[:, None]
        masked = jnp.where(allowed, scores, -1e30)
        new_max = jnp.maximum(run_max, jnp.max(masked, axis=-1))
        weights = jnp.where(allowed, jnp.exp(masked - new_max[..., None]), 0.0)
        rescale = jnp.exp(run_max - new_max)
        new_total = run_total * rescale + jnp.sum(weights, axis=-1)
        product = jnp.einsum(
            "hmqk,khd->hmqd",
            weights.astype(jnp.bfloat16),
            value_block,
            preferred_element_type=jnp.float32,
        )
        return (new_max, new_total, run_accum * rescale[..., None] + product)

    def visit(inner):
        return lax.fori_loop(0, count // block, one_block, inner)

    def keep_carry(inner):
        return inner

    maxima, totals, accum = lax.cond(
        jnp.int32(0) <= first_pos + tok_rows - 1, visit, keep_carry, initial
    )
    log_totals = maxima + jnp.log(totals)
    head_raw = (
        accum[:, 0] / totals[:, 0, :, None]
        - mix_weight[:, None, None] * accum[:, 1] / totals[:, 1, :, None]
    )
    normed_heads = (
        head_raw
        * lax.rsqrt(jnp.mean(head_raw * head_raw, axis=-1, keepdims=True) + 1e-05)
        * head_gain
    )
    attn_out = (
        normed_heads.transpose(1, 0, 2)
        .reshape(tok_rows, head_count * value_dim)
        .astype(jnp.bfloat16)
    )
    return (attn_out, log_totals)


def per_device(
    tokens,
    norm_gain,
    w_state_in,
    w_query,
    w_key,
    w_value,
    decay_re,
    decay_im,
    log_step,
    decay_shift,
    in_re,
    in_im,
    output_real,
    output_imaginary,
    skip,
    mix_weight,
    head_gain,
    w_out_state,
    w_out_attn,
):
    whole = lax.all_gather(tokens, "tp", axis=2, tiled=True)[0]
    floats = whole.astype(jnp.float32)
    normed = (
        floats * lax.rsqrt(jnp.mean(floats * floats, axis=-1, keepdims=True) + 1e-06) * norm_gain
    ).astype(jnp.bfloat16)
    pieces = (
        lax.all_gather(w_state_in, ("sp", "fs"), axis=0, tiled=True),
        lax.all_gather(w_query, ("sp", "fs"), axis=0, tiled=True),
        lax.all_gather(w_key, ("sp", "fs"), axis=0, tiled=True),
        lax.all_gather(w_value, ("sp", "fs"), axis=0, tiled=True),
    )
    sums = tuple((jnp.dot(normed, piece, preferred_element_type=jnp.float32) for piece in pieces))
    state_in = sums[0].astype(jnp.bfloat16)
    queries = sums[1].astype(jnp.bfloat16)
    keys_local = sums[2].astype(jnp.bfloat16)
    values_local = sums[3].astype(jnp.bfloat16)
    attn_out, log_totals = attention_branch(
        queries, keys_local, values_local, mix_weight, head_gain
    )
    state_out = state_branch(
        state_in,
        decay_re,
        decay_im,
        log_step,
        decay_shift,
        in_re,
        in_im,
        output_real,
        output_imaginary,
        skip,
    )
    summed = lax.psum_scatter(
        (
            jnp.dot(state_out, w_out_state, preferred_element_type=jnp.float32)
            + jnp.dot(attn_out, w_out_attn, preferred_element_type=jnp.float32)
        ).astype(jnp.bfloat16),
        "tp",
        scatter_dimension=0,
        tiled=True,
    )
    return (summed[None], log_totals[None])


def nt_dot(a, b):
    return lax.dot_general(a, b, (((1,), (1,)), ((), ())), preferred_element_type=jnp.float32)


def split_pair(x):
    high = x.astype(jnp.bfloat16)
    low = (x - high.astype(jnp.float32)).astype(jnp.bfloat16)
    return (high, low)


def small_expm1(x):
    total = jnp.ones_like(x)
    for n in range(9, 1, -1):
        total = 1.0 + total * x * (1.0 / n)
    return total * x


def fused_kernel(
    sizes,
    tok_ref,
    gain_ref,
    ws_ref,
    wq_ref,
    wk_ref,
    wv_ref,
    dre_ref,
    dim_ref,
    logstep_ref,
    shift_ref,
    inre_ref,
    inim_ref,
    outre_ref,
    outim_ref,
    skip_ref,
    mix_ref,
    hgain_ref,
    wos_ref,
    woa_ref,
    mixed_ref,
    logt_ref,
    stat_send,
    stat_recv,
    nbuf,
    xbuf,
    wbuf,
    pbuf,
    rbuf,
    fin,
    shsend,
    shbuf,
    inbuf,
    outbuf,
    coef,
    etab,
    bcat,
    ccat,
    srow,
    yacc,
    wts,
    stb,
    atb,
    sto,
    ato,
    ltb,
    lto,
    wo,
    acc,
    poutb,
    precb,
    loc_sem,
    wo_sem,
    w_loc,
    stat_sem,
    tok_send,
    tok_recv,
    fwd_send,
    wx_send,
    wx_recv,
    wy_send,
    wy_recv,
    dx_send,
    dx_recv,
    dy_send,
    dy_recv,
    z_send,
    zr_recv,
    zl_recv,
    sh_send,
    sh_recv,
    st_send,
    st_recv,
    at_send,
    at_recv,
    lt_send,
    lt_recv,
    p_send,
    p_recv,
):
    NS, NT, L, D, CW = sizes
    KW = D // NS
    FW = D // NT
    NB = NS // NT
    HC = CW // NS
    SEQ = NS * L
    G = HC // 16
    MESH = pl.DeviceIdType.MESH
    s, f, c = (lax.axis_index("sp"), lax.axis_index("fs"), lax.axis_index("tp"))
    fx = f + 1 - 2 * lax.rem(f, 2)
    fy = lax.rem(f + 2, 4)
    fd = 3 - f
    partner = {"tp": 1 - c}
    owner = s // NB

    def remote(src, dst, send, recv, where):
        return pltpu.make_async_remote_copy(
            src_ref=src, dst_ref=dst, send_sem=send, recv_sem=recv, device_id=where, device_id_type=MESH
        )

    g0 = pl.multiple_of(s * G, G)
    own_w = [
        pltpu.make_async_copy(ref, wbuf.at[m, f], w_loc.at[m])
        for m, ref in enumerate((ws_ref, wq_ref, wk_ref, wv_ref))
    ]
    for copy in own_w:
        copy.start()
    own_p = [
        pltpu.make_async_copy(ref.at[pl.ds(g0, G)], dst, loc_sem.at[i])
        for i, (ref, dst) in enumerate(
            (
                (inre_ref, inbuf.at[0]),
                (inim_ref, inbuf.at[1]),
                (outre_ref, outbuf.at[0]),
                (outim_ref, outbuf.at[1]),
            )
        )
    ]
    for copy in own_p:
        copy.start()
    big = [pltpu.make_async_copy(ref, wo.at[i], wo_sem.at[i]) for i, ref in enumerate((wos_ref, woa_ref))]
    for copy in big:
        copy.start()

    barrier = pltpu.get_barrier_semaphore()
    pl.semaphore_signal(barrier, inc=1, device_id={"fs": fx}, device_id_type=MESH)
    pl.semaphore_signal(barrier, inc=1, device_id={"fs": fy}, device_id_type=MESH)
    pl.semaphore_signal(barrier, inc=1, device_id=partner, device_id_type=MESH)
    for k in range(1, NS):
        pl.semaphore_signal(barrier, inc=1, device_id={"sp": lax.rem(s + k, NS)}, device_id_type=MESH)
    pl.semaphore_wait(barrier, 2 + NS)

    def own_x(m):
        return remote(wbuf.at[m, f], wbuf.at[m, f], wx_send.at[m], wx_recv.at[m], {"fs": fx})

    def own_y(m):
        return remote(wbuf.at[m, f], wbuf.at[m, f], wy_send.at[m], wy_recv.at[m], {"fs": fy})

    half = wbuf.shape[2] // 2

    def fwd_y(m):
        part = wbuf.at[m, fx, pl.ds(0, half)]
        return remote(part, part, dy_send.at[m], dy_recv.at[m], {"fs": fy})

    def fwd_x(m):
        part = wbuf.at[m, fy, pl.ds(half, half)]
        return remote(part, part, dx_send.at[m], dx_recv.at[m], {"fs": fx})

    tokens = tok_ref[0].astype(jnp.float32)
    square = jnp.sum(tokens * tokens, axis=1, keepdims=True)
    stat_send[...] = jnp.broadcast_to(square, (L, 128))
    stat = remote(stat_send, stat_recv, stat_sem.at[0], stat_sem.at[1], partner)
    stat.start()
    for m in range(4):
        own_w[m].wait()
    for m in range(2):
        own_x(m).start()
        own_y(m).start()
    for d in range(NS):
        shsend[d] = shift_ref[0, d * G : (d + 1) * G, :]
    for k in range(1, NS):
        d = lax.rem(s + k, NS)
        remote(shsend.at[d], shbuf.at[s], sh_send.at[d], sh_recv.at[s], {"sp": d}).start()
    shbuf[s] = shsend[s]
    stat.wait()
    mean = (square + stat_recv[:, 0:1]) * (1.0 / D)
    gain = gain_ref[:, pl.ds(pl.multiple_of(c * FW, FW), FW)]
    normed = (tok_ref[0].astype(jnp.float32) * lax.rsqrt(mean + 1e-06) * gain).astype(jnp.bfloat16)

    def tok_copy(i):
        return remote(
            nbuf.at[i], xbuf.at[s], tok_send.at[i], tok_recv.at[s], {"sp": c * NB + i}
        )

    for i in range(NB):
        nbuf[i] = normed[:, i * KW : (i + 1) * KW]
    for i in range(NB):
        @pl.when(c * NB + i != s)
        def _():
            tok_copy(i).start()

        @pl.when(c * NB + i == s)
        def _():
            xbuf[s] = nbuf[i]

    def tok_forward(q):
        return remote(xbuf.at[q], xbuf.at[q], fwd_send.at[q], tok_recv.at[q], partner)

    def tok_arrival(q):
        return remote(xbuf.at[q], xbuf.at[q], fwd_send.at[q], tok_recv.at[q], partner)

    re16 = dre_ref[pl.ds(g0, G), :]
    im16 = dim_ref[pl.ds(g0, G), :]
    re16 = jnp.concatenate([re16, re16], axis=1)
    im16 = jnp.concatenate([im16, im16], axis=1)
    numer_re = small_expm1(re16) * jnp.cos(im16) - 2.0 * jnp.sin(0.5 * im16) ** 2
    numer_im = jnp.exp(re16) * jnp.sin(im16)
    modulus = re16 * re16 + im16 * im16
    coef[0] = re16
    coef[1] = im16
    coef[2] = (numer_re * re16 + numer_im * im16) / modulus
    coef[3] = (numer_im * re16 - numer_re * im16) / modulus
    for copy in own_p:
        copy.wait()
    lane = lax.broadcasted_iota(jnp.int32, (128, 16), 0)
    chan = lax.broadcasted_iota(jnp.int32, (128, 16), 1)
    steps = lax.broadcasted_iota(jnp.int32, (L, 128), 0).astype(jnp.float32) + 1.0
    sel_hi = lax.broadcasted_iota(jnp.int32, (128, 16), 0)

    def table(g, carry):
        zr = coef[0, pl.ds(g, 1), :]
        zi = coef[1, pl.ds(g, 1), :]
        step = jnp.exp(jnp.full((1, 128), logstep_ref[g0 + g], jnp.float32))
        cr = coef[2, pl.ds(g, 1), :] * step
        ci = coef[3, pl.ds(g, 1), :] * step
        angle = steps * zi
        cosine, sine = (jnp.cos(angle), jnp.sin(angle))
        shrink = jnp.exp(steps * zr)
        grow = jnp.exp(-(steps * zr))
        etab[0, g] = grow * (cosine * cr + sine * ci)
        etab[1, g] = grow * (cosine * ci - sine * cr)
        etab[2, g] = shrink * cosine
        etab[3, g] = shrink * sine
        pick = (lane == lax.rem(g, 8) * 16 + chan).astype(jnp.bfloat16)
        ir, ii = (inbuf[0, g], inbuf[1, g])
        raw = jnp.concatenate([ir, ii, -ii, ir], axis=1)
        hi, lo = split_pair(raw)
        bcat[g] = jnp.concatenate(
            [
                jnp.dot(pick, hi, preferred_element_type=jnp.float32).astype(jnp.bfloat16),
                jnp.dot(pick, lo, preferred_element_type=jnp.float32).astype(jnp.bfloat16),
            ],
            axis=0,
        )
        cr_, ci_ = (outbuf[0, g], outbuf[1, g])
        rawc = jnp.concatenate([cr_, -ci_, -ci_, -cr_], axis=1)
        hi, lo = split_pair(rawc)
        ccat[g] = jnp.concatenate(
            [
                jnp.dot(pick, hi, preferred_element_type=jnp.float32).astype(jnp.bfloat16),
                jnp.dot(pick, lo, preferred_element_type=jnp.float32).astype(jnp.bfloat16),
            ],
            axis=0,
        )
        return carry

    lax.fori_loop(0, G, table, 0)
    for k in range(1, NS):
        q = lax.rem(s + k, NS)
        remote(shsend.at[q], shbuf.at[q], sh_send.at[q], sh_recv.at[q], {"sp": q}).wait_recv()
    row_i = lax.broadcasted_iota(jnp.int32, (L, L), 0)
    col_i = lax.broadcasted_iota(jnp.int32, (L, L), 1)
    upper = (row_i <= col_i).astype(jnp.float32)
    for k in range(NS):
        srow[k] = jnp.dot(
            shbuf[k], upper, precision=lax.Precision.HIGHEST, preferred_element_type=jnp.float32
        )

    for k in range(NS):
        q = lax.rem(s + k, NS)

        @pl.when(c == owner)
        def _():
            @pl.when(q != s)
            def _():
                tok_arrival(q).wait_recv()

            tok_forward(q).start()

        @pl.when(c != owner)
        def _():
            tok_arrival(q).wait_recv()

    def z_right(m, d):
        return remote(pbuf.at[m, d], rbuf.at[0, m, d], z_send.at[m, d], zr_recv.at[m, d], {"sp": lax.rem(s + 1, NS)})

    def z_left(m, d):
        return remote(
            pbuf.at[m, d], rbuf.at[1, m, d], z_send.at[m, d], zl_recv.at[m, d], {"sp": lax.rem(s + NS - 1, NS)}
        )

    def hop_right(m, k):
        d = NS - 1 - k

        @pl.when(d > s)
        def _():
            z_right(m, d).wait_recv()
            pbuf[m, d] = (pbuf[m, d].astype(jnp.float32) + rbuf[0, m, d].astype(jnp.float32)).astype(jnp.bfloat16)
            z_right(m, d).start()

    def hop_left(m, d):
        @pl.when(d < s)
        def _():
            z_left(m, d).wait_recv()
            pbuf[m, d] = (pbuf[m, d].astype(jnp.float32) + rbuf[1, m, d].astype(jnp.float32)).astype(jnp.bfloat16)
            z_left(m, d).start()

    def each(hop, m):
        def one(k, carry):
            hop(m, k)
            return carry

        lax.fori_loop(0, NS, one, 0)

    def relay(m):
        @pl.when(jnp.logical_and(s > 0, s < NS // 2))
        def _():
            each(hop_right, m)
            each(hop_left, m)

        @pl.when(jnp.logical_and(s >= NS // 2, s < NS - 1))
        def _():
            each(hop_left, m)
            each(hop_right, m)


    def project(m, carry):
        own_x(m).wait_recv()
        own_y(m).wait_recv()
        fwd_y(m).start()
        fwd_x(m).start()

        @pl.when(m < 2)
        def _():
            own_x(m + 2).start()
            own_y(m + 2).start()

        @pl.when(m > 0)
        def _():
            relay(m - 1)

        diag_y = wbuf.at[m, fd, pl.ds(0, half)]
        diag_x = wbuf.at[m, fd, pl.ds(half, half)]
        remote(diag_y, diag_y, dy_send.at[m], dy_recv.at[m], {"fs": fy}).wait_recv()
        remote(diag_x, diag_x, dx_send.at[m], dx_recv.at[m], {"fs": fx}).wait_recv()

        def block(k, inner):
            d = jnp.where(s < NS // 2, NS - 1 - k, k)
            columns = pl.ds(pl.multiple_of(d * HC, HC), HC)
            lhs = xbuf[...].reshape(SEQ, KW)
            rhs = wbuf[m, :, :, columns].reshape(KW, HC)
            part = jnp.dot(lhs, rhs, preferred_element_type=jnp.float32).astype(jnp.bfloat16)

            pbuf[m, d] = part

            @pl.when(jnp.logical_and(s == 0, d > 0))
            def _():
                z_right(m, d).start()

            @pl.when(jnp.logical_and(s == NS - 1, d < NS - 1))
            def _():
                z_left(m, d).start()

            return inner

        return lax.fori_loop(0, NS, block, carry)

    def finish(m):
        @pl.when(s > 0)
        def _():
            z_right(m, s).wait_recv()

        @pl.when(s < NS - 1)
        def _():
            z_left(m, s).wait_recv()

        own = pbuf[m, s].astype(jnp.float32)

        @pl.when(s == 0)
        def _():
            fin[m] = (own + rbuf[1, m, s].astype(jnp.float32)).astype(jnp.bfloat16)

        @pl.when(s == NS - 1)
        def _():
            fin[m] = (own + rbuf[0, m, s].astype(jnp.float32)).astype(jnp.bfloat16)

        @pl.when(jnp.logical_and(s > 0, s < NS - 1))
        def _():
            fin[m] = (own + rbuf[0, m, s].astype(jnp.float32) + rbuf[1, m, s].astype(jnp.float32)).astype(jnp.bfloat16)

    lax.fori_loop(0, 3, project, 0)

    finish(0)
    sign = jnp.where(lax.broadcasted_iota(jnp.int32, (8, 128), 1) < 64, -1.0, 1.0)
    lower = row_i >= col_i

    def lane_block(b, carry):
        lanes = pl.ds(pl.multiple_of(b * 128, 128), 128)
        u = fin[0, :, lanes]
        uu = jnp.concatenate([u, u], axis=1)
        yacc[...] = jnp.zeros_like(yacc)

        def group(g8, inner):
            g = b * 8 + g8
            drives = jnp.dot(uu, bcat[g], preferred_element_type=jnp.float32)
            h = jnp.zeros((1, 128), jnp.float32)
            er, ei, fr, fi = (etab[0, g], etab[1, g], etab[2, g], etab[3, g])
            for k in range(NS):
                d = drives[k * L : (k + 1) * L]
                x = er * d[:, :128] + ei * d[:, 128:]
                xh, xl = split_pair(x)
                xx = jnp.concatenate([xh, xl], axis=1)
                rhs = jnp.concatenate([xx, xx], axis=0)
                sr = jnp.broadcast_to(srow[k, pl.ds(g, 1), :], (L, L))
                sc = sr.T
                mask = jnp.where(lower, jnp.exp(jnp.minimum(sc - sr, 0.0)), 0.0)
                mh, ml = split_pair(mask)
                w2 = jnp.dot(
                    jnp.concatenate([mh, ml], axis=1), rhs, preferred_element_type=jnp.float32
                )
                q = w2[:, :128] + w2[:, 128:] + jnp.exp(sc) * h
                p1 = q * fr
                p2 = q * fi
                tail = p1[L - 8 :] + sign * pltpu.roll(p2[L - 8 :], 64, 1)
                h = tail[7:8]
                ph, plow = split_pair(jnp.concatenate([p1, p2], axis=1))
                y2 = nt_dot(ph, ccat[g]) + nt_dot(plow, ccat[g])
                yacc[k * L : (k + 1) * L, :] += y2[:, :128] + y2[:, 128:]
            return inner

        lax.fori_loop(0, 8, group, 0)
        direct = skip_ref[:, pl.ds(pl.multiple_of(s * HC + b * 128, 128), 128)]
        out = (yacc[...] + direct * u.astype(jnp.float32)).astype(jnp.bfloat16)
        for k in range(NS):
            stb[k, :, lanes] = out[k * L : (k + 1) * L]
        return carry

    lax.fori_loop(0, HC // 128, lane_block, 0)

    lax.fori_loop(3, 4, project, 0)

    def st_copy(d):
        return remote(stb.at[d], sto.at[s], st_send.at[d], st_recv.at[s], {"sp": d})

    def at_copy(d):
        return remote(atb.at[d], ato.at[s], at_send.at[d], at_recv.at[s], {"sp": d})

    def lt_copy(d):
        return remote(ltb.at[d], lto.at[s], lt_send.at[d], lt_recv.at[s], {"sp": d})

    for k in range(1, NS):
        st_copy(lax.rem(s + k, NS)).start()
    sto[s] = stb[s]

    hd = HC // 2
    relay(3)
    finish(1)
    finish(2)
    lam = mix_ref[s]
    totals = []
    for i in range(NS):
        width = (i + 1) * L
        for m in range(2):
            sc = nt_dot(
                fin[1, i * L : (i + 1) * L, m * hd : (m + 1) * hd], fin[2, 0:width, m * hd : (m + 1) * hd]
            ) * (hd ** (-0.5))
            qpos = lax.broadcasted_iota(jnp.int32, (L, width), 0) + i * L
            kpos = lax.broadcasted_iota(jnp.int32, (L, width), 1)
            allowed = kpos <= qpos
            sc = jnp.where(allowed, sc, -1e30)
            top = jnp.max(sc, axis=1, keepdims=True)
            weights = jnp.where(allowed, jnp.exp(sc - top), 0.0)
            total = jnp.sum(weights, axis=1, keepdims=True)
            wts[m, i * L : (i + 1) * L, 0:width] = weights.astype(jnp.bfloat16)
            totals.append(1.0 / total)
            logs = jnp.broadcast_to(top + jnp.log(total), (L, L)).T
            ltb[i, m : m + 1, :] = logs[0:1]
    for k in range(1, NS):
        lt_copy(lax.rem(s + k, NS)).start()
    lto[s] = ltb[s]
    finish(3)
    for i in range(NS):
        width = (i + 1) * L
        heads = [
            jnp.dot(
                wts[m, i * L : (i + 1) * L, 0:width], fin[3, 0:width, :], preferred_element_type=jnp.float32
            )
            * totals[2 * i + m]
            for m in range(2)
        ]
        raw = heads[0] - lam * heads[1]
        scale = lax.rsqrt(jnp.mean(raw * raw, axis=1, keepdims=True) + 1e-05)
        atb[i] = (raw * scale * hgain_ref[...]).astype(jnp.bfloat16)

    for k in range(1, NS):
        d = lax.rem(s + k, NS)
        at_copy(d).start()
    ato[s] = atb[s]

    for copy in big:
        copy.wait()
    for k in range(1, NS):
        q = lax.rem(s + k, NS)
        remote(stb.at[q], sto.at[q], st_send.at[q], st_recv.at[q], {"sp": q}).wait_recv()
    tiles = poutb.shape[0]
    width = D // tiles
    st_lhs = jnp.concatenate([sto[q] for q in range(NS)], axis=1)

    def state_tile(n, carry):
        columns = pl.ds(pl.multiple_of(n * width, width), width)
        acc[:, columns] = jnp.dot(st_lhs, wo[0, :, columns], preferred_element_type=jnp.float32)
        return carry

    lax.fori_loop(0, tiles, state_tile, 0)
    for k in range(1, NS):
        q = lax.rem(s + k, NS)
        remote(atb.at[q], ato.at[q], at_send.at[q], at_recv.at[q], {"sp": q}).wait_recv()
    at_lhs = jnp.concatenate([ato[q] for q in range(NS)], axis=1)
    rows = L // NT
    mine = pl.ds(pl.multiple_of(c * rows, rows), rows)

    def p_copy(n):
        theirs = pl.ds(pl.multiple_of((1 - c) * rows, rows), rows)
        return remote(poutb.at[n, theirs], precb.at[n], p_send.at[n], p_recv.at[n], partner)

    def attn_tile(n, carry):
        columns = pl.ds(pl.multiple_of(n * width, width), width)
        part = acc[:, columns] + jnp.dot(at_lhs, wo[1, :, columns], preferred_element_type=jnp.float32)
        poutb[n] = part.astype(jnp.bfloat16)
        p_copy(n).start()
        return carry

    lax.fori_loop(0, tiles, attn_tile, 0)

    def last_tile(n, carry):
        columns = pl.ds(pl.multiple_of(n * width, width), width)
        p_copy(n).wait()
        mixed_ref[0, :, columns] = (
            poutb[n, mine, :].astype(jnp.float32) + precb[n].astype(jnp.float32)
        ).astype(jnp.bfloat16)
        return carry

    lax.fori_loop(0, tiles, last_tile, 0)
    for k in range(1, NS):
        q = lax.rem(s + k, NS)
        remote(ltb.at[q], lto.at[q], lt_send.at[q], lt_recv.at[q], {"sp": q}).wait_recv()
    logt_ref[0] = lto[...]

    for m in range(4):
        own_x(m).wait_send()
        own_y(m).wait_send()
        fwd_x(m).wait_send()
        fwd_y(m).wait_send()
        for k in range(1, NS):
            z_right(m, lax.rem(s + k, NS)).wait_send()
    for k in range(1, NS):
        d = lax.rem(s + k, NS)
        remote(shsend.at[d], shbuf.at[s], sh_send.at[d], sh_recv.at[s], {"sp": d}).wait_send()
        st_copy(d).wait_send()
        at_copy(d).wait_send()
        lt_copy(d).wait_send()
    for i in range(NB):
        @pl.when(c * NB + i != s)
        def _():
            tok_copy(i).wait_send()

    @pl.when(c == owner)
    def _():
        for q in range(NS):
            tok_forward(q).wait_send()


def fused_device(sizes, *args):
    (tokens, norm_gain, ws, wq, wk, wv, dre, dim, logstep, shift, inre, inim, outre, outim, skip, mix, hgain, wos, woa) = args
    NS, NT, L, D, CW = sizes
    KW, HC = (D // NS, CW // NS)
    SEQ, G, NB, NF = (NS * L, HC // 16, NS // NT, 4)
    tiles = 8
    bf, f32 = (jnp.bfloat16, jnp.float32)
    V = pltpu.VMEM
    DMA = pltpu.SemaphoreType.DMA
    vmem = pl.BlockSpec(memory_space=pltpu.VMEM)
    smem = pl.BlockSpec(memory_space=pltpu.SMEM)
    hbm = pl.BlockSpec(memory_space=pl.ANY)
    scratch = [
        V((L, 128), f32),
        V((L, 128), f32),
        V((NB, L, KW), bf),
        V((NS, L, KW), bf),
        V((4, NF, ws.shape[0], CW), bf),
        V((4, NS, SEQ, HC), bf),
        V((2, 4, NS, SEQ, HC), bf),
        V((4, SEQ, HC), bf),
        V((NS, G, L), f32),
        V((NS, G, L), f32),
        V((2, G, 16, 64), f32),
        V((2, G, 16, 64), f32),
        V((4, G, 128), f32),
        V((4, G, L, 128), f32),
        V((G, 256, 256), bf),
        V((G, 256, 256), bf),
        V((NS, G, L), f32),
        V((SEQ, 128), f32),
        V((2, SEQ, SEQ), bf),
        V((NS, L, HC), bf),
        V((NS, L, HC), bf),
        V((NS, L, HC), bf),
        V((NS, L, HC), bf),
        V((NS, 2, L), f32),
        V((NS, 2, L), f32),
        V((2, CW, D), bf),
        V((L, D), f32),
        V((tiles, L, D // tiles), bf),
        V((tiles, L // NT, D // tiles), bf),
        DMA((4,)),
        DMA((2,)),
        DMA((4,)),
        DMA((2,)),
        DMA((NB,)),
        DMA((NS,)),
        DMA((NS,)),
    ]
    scratch += [DMA((4,))] * 8
    scratch += [DMA((4, NS))] * 3
    scratch += [DMA((NS,))] * 8
    scratch += [DMA((tiles,))] * 2
    call = pl.pallas_call(
        functools.partial(fused_kernel, sizes),
        out_shape=(
            jax.ShapeDtypeStruct((1, L // NT, D), bf),
            jax.ShapeDtypeStruct((1, NS, 2, L), f32),
        ),
        in_specs=[vmem, vmem, hbm, hbm, hbm, hbm, vmem, vmem, smem, vmem, hbm, hbm, hbm, hbm, vmem, smem, vmem, hbm, hbm],
        out_specs=(vmem, vmem),
        scratch_shapes=scratch,
        compiler_params=pltpu.CompilerParams(
            collective_id=0, has_side_effects=True, vmem_limit_bytes=67043328
        ),
    )
    return call(
        tokens, norm_gain.reshape(1, -1), ws, wq, wk, wv, dre, dim, logstep, shift,
        inre.transpose(0, 2, 1), inim.transpose(0, 2, 1), outre, outim,
        skip.reshape(1, -1), mix, hgain.reshape(1, -1), wos, woa,
    )


def choose_device(sp, fs, tp, *args):
    tokens, ws, dre, inre, mix = (args[0], args[2], args[6], args[10], args[15])
    L, D = (tokens.shape[1], ws.shape[0] * sp * fs)
    CW = ws.shape[1]
    fits = (
        fs == 4
        and tp == 2
        and sp % tp == 0
        and mix.shape[0] == sp
        and L == 128
        and CW == sp * 256
        and dre.shape == (sp * 16, 64)
        and inre.shape[2] == 16
        and D % (sp * 128) == 0
    )
    if fits:
        return fused_device((sp, tp, L, D, CW), *args)
    return per_device(*args)


def solution(mesh):
    in_specs = (
        P("fs", "sp", "tp"),
        P(),
        P(("sp", "fs"), "tp"),
        P(("sp", "fs"), "tp"),
        P(("sp", "fs"), "tp"),
        P(("sp", "fs"), "tp"),
        P("tp", None),
        P("tp", None),
        P("tp"),
        P("fs", "tp", "sp"),
        P("tp", None, None),
        P("tp", None, None),
        P("tp", None, None),
        P("tp", None, None),
        P("tp"),
        P("tp"),
        P(),
        P("tp", None),
        P("tp", None),
    )
    out_specs = (P("fs", ("sp", "tp"), None), P("fs", "tp", None, "sp"))
    body = functools.partial(choose_device, mesh.shape["sp"], mesh.shape["fs"], mesh.shape["tp"])
    return jax.shard_map(
        body, mesh=mesh, in_specs=in_specs, out_specs=out_specs, check_vma=False
    )
```

profile of v0, /device:TPU:1, one launch (start us, length us, event | category | flops | bytes accessed | tf_op | source)
XLA Modules:
  0.0 136.3 jit_solution(17276707903534837685)
XLA Ops:
  0.6 132.6 %shard_map.194 = (bf16[1,64,4096]{2,1,0:T(8,128)(2,1)}, f32[1,4,2,128]{3,2,1,0:T(2,128)}) custom-call(bf16[1,128,2048]{2,1,0:T(8,128)(2,1)} %tok_ref.1, f32[1,4096]{1,0:T(1,128)} %bitcast.7, bf16[256,1024]{1,0:T(8,128)(2,1)} %ws_ref.1, bf16[256,1024]{1,0:T(8,128)(2,1)} %wq_ref.1, bf16[256,1024]{1,0:T(8,128)(2,1)} %wk_ref.1, bf16[256,1024]{1,0:T(8,128)(2,1)} %wv_ref.1, ...), custom_call_target="tpu_custom_call" | custom-call | tf_op jit(solution)/shard_map/pallas_call | solution.py:901
  133.2 1.9 %copy.23 = bf16[1,64,4096]{2,1,0:T(8,128)(2,1)} copy(bf16[1,64,4096]{2,1,0:T(8,128)(2,1)} %get-tuple-element.4) | data formatting | bytes 1048576
  135.1 1.3 copy.24
where the time goes:
time: 137 us; the launch traced here: 136 us
  Pallas kernels  133 us (97%)
  local copies, waits for them, and re-layouts  3.13 us (2%)
    pallas_call x1, Pallas kernels, fused_device(): call(tokens, norm_gain.reshape(1, -1), ws, wq, wk, wv, dre, dim, logstep,...  133 us
    unnamed x2, local copies, waits for them, and re-layouts  3.13 us

commit v1 on v0

--- a/solution.py
+++ b/solution.py
@@ -295,9 +295,11 @@
     stat_recv,
     nbuf,
     xbuf,
+    wl,
     wbuf,
-    pbuf,
-    rbuf,
+    ykeep,
+    ysend,
+    yrecv,
     fin,
     shsend,
     shbuf,
@@ -323,21 +325,18 @@
     loc_sem,
     wo_sem,
     w_loc,
+    w_own,
     stat_sem,
-    tok_send,
-    tok_recv,
-    fwd_send,
-    wx_send,
-    wx_recv,
+    x_src,
+    x_part,
+    x_cross,
+    x_rel,
+    x_recv,
+    wd_send,
     wy_send,
-    wy_recv,
-    dx_send,
-    dx_recv,
-    dy_send,
-    dy_recv,
-    z_send,
-    zr_recv,
-    zl_recv,
+    w_recv,
+    y_send,
+    y_recv,
     sh_send,
     sh_recv,
     st_send,
@@ -350,29 +349,45 @@
     p_recv,
 ):
     NS, NT, L, D, CW = sizes
-    KW = D // NS
+    KW = D // 2
+    KB = D // (NS * 4)
     FW = D // NT
-    NB = NS // NT
     HC = CW // NS
     SEQ = NS * L
     G = HC // 16
     MESH = pl.DeviceIdType.MESH
     s, f, c = (lax.axis_index("sp"), lax.axis_index("fs"), lax.axis_index("tp"))
-    fx = f + 1 - 2 * lax.rem(f, 2)
+    zh, zl = (s // 2, lax.rem(s, 2))
+    y, x = (f // 2, lax.rem(f, 2))
+    s1 = s + 1 - 2 * zl
+    s2 = lax.rem(s + 2, NS)
+    fx = f + 1 - 2 * x
     fy = lax.rem(f + 2, 4)
     fd = 3 - f
+    keep = zh + x - 2 * zh * x
+    give = 1 - keep
+    hq = 2 * x + zl
+    home = 2 * y + keep
     partner = {"tp": 1 - c}
-    owner = s // NB
 
     def remote(src, dst, send, recv, where):
         return pltpu.make_async_remote_copy(
             src_ref=src, dst_ref=dst, send_sem=send, recv_sem=recv, device_id=where, device_id_type=MESH
         )
 
-    g0 = pl.multiple_of(s * G, G)
+    g0 = pl.multiple_of(hq * G, G)
+    kbo = zl * 4 + f
+
+    def head_columns(h):
+        return pl.ds(pl.multiple_of(h * HC, HC), HC)
+
+    w_refs = (ws_ref, wq_ref, wk_ref, wv_ref)
+    load_w = [pltpu.make_async_copy(ref, wl.at[m], w_loc.at[m]) for m, ref in enumerate(w_refs)]
+    for copy in load_w:
+        copy.start()
     own_w = [
-        pltpu.make_async_copy(ref, wbuf.at[m, f], w_loc.at[m])
-        for m, ref in enumerate((ws_ref, wq_ref, wk_ref, wv_ref))
+        pltpu.make_async_copy(ref.at[:, head_columns(hq)], wbuf.at[m, kbo], w_own.at[m])
+        for m, ref in enumerate(w_refs)
     ]
     for copy in own_w:
         copy.start()
@@ -394,71 +409,166 @@
         copy.start()
 
     barrier = pltpu.get_barrier_semaphore()
-    pl.semaphore_signal(barrier, inc=1, device_id={"fs": fx}, device_id_type=MESH)
     pl.semaphore_signal(barrier, inc=1, device_id={"fs": fy}, device_id_type=MESH)
-    pl.semaphore_signal(barrier, inc=1, device_id=partner, device_id_type=MESH)
-    for k in range(1, NS):
-        pl.semaphore_signal(barrier, inc=1, device_id={"sp": lax.rem(s + k, NS)}, device_id_type=MESH)
-    pl.semaphore_wait(barrier, 2 + NS)
-
-    def own_x(m):
-        return remote(wbuf.at[m, f], wbuf.at[m, f], wx_send.at[m], wx_recv.at[m], {"fs": fx})
-
-    def own_y(m):
-        return remote(wbuf.at[m, f], wbuf.at[m, f], wy_send.at[m], wy_recv.at[m], {"fs": fy})
-
-    half = wbuf.shape[2] // 2
-
-    def fwd_y(m):
-        part = wbuf.at[m, fx, pl.ds(0, half)]
-        return remote(part, part, dy_send.at[m], dy_recv.at[m], {"fs": fy})
-
-    def fwd_x(m):
-        part = wbuf.at[m, fy, pl.ds(half, half)]
-        return remote(part, part, dx_send.at[m], dx_recv.at[m], {"fs": fx})
-
+    for k in range(NS):
+        for there in (f, fx):
+            for core in (c, 1 - c):
+                if k == 0 and there is f and core is c:
+                    continue
+                pl.semaphore_signal(
+                    barrier,
+                    inc=1,
+                    device_id={"sp": lax.rem(s + k, NS), "fs": there, "tp": core},
+                    device_id_type=MESH,
+                )
     tokens = tok_ref[0].astype(jnp.float32)
     square = jnp.sum(tokens * tokens, axis=1, keepdims=True)
     stat_send[...] = jnp.broadcast_to(square, (L, 128))
+    pl.semaphore_wait(barrier, 4 * NS)
     stat = remote(stat_send, stat_recv, stat_sem.at[0], stat_sem.at[1], partner)
     stat.start()
-    for m in range(4):
-        own_w[m].wait()
-    for m in range(2):
-        own_x(m).start()
-        own_y(m).start()
-    for d in range(NS):
-        shsend[d] = shift_ref[0, d * G : (d + 1) * G, :]
-    for k in range(1, NS):
-        d = lax.rem(s + k, NS)
-        remote(shsend.at[d], shbuf.at[s], sh_send.at[d], sh_recv.at[s], {"sp": d}).start()
-    shbuf[s] = shsend[s]
+
+    direct = (
+        ((1 - x) * 2 + zl, {"fs": fx}),
+        (x * 2 + 1 - zl, {"sp": s1}),
+        ((1 - x) * 2 + 1 - zl, {"sp": s1, "fs": fx}),
+    )
+    arrive = (zl * 4 + fx, (1 - zl) * 4 + f, (1 - zl) * 4 + fx)
+    across = (zl * 4 + fy, zl * 4 + fd, (1 - zl) * 4 + fy, (1 - zl) * 4 + fd)
+
+    def w_direct(m, j):
+        h, where = direct[j]
+        return remote(
+            wl.at[m, :, head_columns(h)], wbuf.at[m, kbo], wd_send.at[m, j], w_recv.at[m, kbo], where
+        )
+
+    def w_own_y(m):
+        return remote(
+            wl.at[m, :, head_columns(hq)], wbuf.at[m, kbo], wy_send.at[m, 3], w_recv.at[m, kbo], {"fs": fy}
+        )
+
+    def w_forward(m, j):
+        part = wbuf.at[m, arrive[j]]
+        return remote(part, part, wy_send.at[m, j], w_recv.at[m, arrive[j]], {"fs": fy})
+
+    def w_arrival(m, kb):
+        part = wbuf.at[m, kb]
+        return remote(part, part, wy_send.at[m, 0], w_recv.at[m, kb], {"fs": fy})
+
+    def start_direct(m):
+        for j in (2, 1, 0):
+            w_direct(m, j).start()
+
+    def forward_all(m):
+        for j in range(3):
+            w_arrival(m, arrive[j]).wait_recv()
+            w_forward(m, j).start()
+
+    def wait_across(m):
+        for kb in across:
+            w_arrival(m, kb).wait_recv()
+
+    load_w[0].wait()
+    start_direct(0)
+    w_own_y(0).start()
+    load_w[1].wait()
+    w_own_y(1).start()
+
+    def shift_copy(xd, zd):
+        zhd = xd + x - 2 * xd * x
+        h = 2 * xd + zd
+        return remote(
+            shsend.at[h], shbuf.at[s], sh_send.at[h], sh_recv.at[s], {"sp": 2 * zhd + zd, "fs": 2 * y + xd}
+        )
+
+    def to_self(xd, zd):
+        return jnp.logical_and(zh == 0, jnp.logical_and(x == xd, zl == zd))
+
+    for h in range(NS):
+        shsend[h] = shift_ref[0, h * G : (h + 1) * G, :]
+    for xd in range(2):
+        for zd in range(2):
+            @pl.when(jnp.logical_not(to_self(xd, zd)))
+            def _():
+                shift_copy(xd, zd).start()
+
+    @pl.when(zh == 0)
+    def _():
+        shbuf[s] = shsend[hq]
+
     stat.wait()
     mean = (square + stat_recv[:, 0:1]) * (1.0 / D)
     gain = gain_ref[:, pl.ds(pl.multiple_of(c * FW, FW), FW)]
     normed = (tok_ref[0].astype(jnp.float32) * lax.rsqrt(mean + 1e-06) * gain).astype(jnp.bfloat16)
-
-    def tok_copy(i):
-        return remote(
-            nbuf.at[i], xbuf.at[s], tok_send.at[i], tok_recv.at[s], {"sp": c * NB + i}
-        )
-
-    for i in range(NB):
-        nbuf[i] = normed[:, i * KW : (i + 1) * KW]
-    for i in range(NB):
-        @pl.when(c * NB + i != s)
+    nbuf[...] = normed
+    mine_half = c == zh
+    q2 = 2 * (1 - zh) + zh
+    order = (s, s1, q2, 2 * (1 - zh) + 1 - zh)
+    duty = (zh, 1 - zh, zh, 1 - zh)
+    near_s = 1 + c
+    first_s = 2 - c
+    near_core = jnp.where(s == first_s, c, 1 - c)
+
+    def x_source(where):
+        return remote(nbuf, xbuf.at[x, s], x_src, x_recv.at[x, s], where)
+
+    far_target = {"sp": near_s, "tp": near_core}
+    pair_target = {"sp": s1, "tp": 1 - zh}
+
+    def x_part_copy(slot, i, q):
+        part = xbuf.at[slot, q]
+        return remote(part, part, x_part.at[slot, i], x_recv.at[slot, q], partner)
+
+    def x_cross_copy(i):
+        part = xbuf.at[x, order[i]]
+        return remote(part, part, x_cross.at[i], x_recv.at[x, order[i]], {"fs": fx})
+
+    def x_relay_copy(i):
+        part = xbuf.at[x, order[i]]
+        return remote(part, part, x_rel.at[i - 2], x_recv.at[x, order[i]], {"sp": s1})
+
+    def x_arrival(slot, q):
+        part = xbuf.at[slot, q]
+        return remote(part, part, x_src, x_recv.at[slot, q], partner)
+
+    relays = zl == 1 - zh
+
+    @pl.when(mine_half)
+    def _():
+        xbuf[x, s] = nbuf[...]
+        x_source(pair_target).start()
+        remote(nbuf, xbuf.at[x, s], x_cross.at[0], x_recv.at[x, s], {"fs": fx}).start()
+        remote(nbuf, xbuf.at[x, s], x_part.at[x, 0], x_recv.at[x, s], partner).start()
+
+    @pl.when(jnp.logical_not(mine_half))
+    def _():
+        x_source(far_target).start()
+
+    def x_own(i):
+        q = order[i]
+        if i == 0:
+            @pl.when(jnp.logical_not(mine_half))
+            def _():
+                x_arrival(x, q).wait_recv()
+            return
+        x_arrival(x, q).wait_recv()
+
+        @pl.when(c == duty[i])
         def _():
-            tok_copy(i).start()
-
-        @pl.when(c * NB + i == s)
+            if i >= 2:
+                @pl.when(relays)
+                def _():
+                    x_relay_copy(i).start()
+            x_cross_copy(i).start()
+            x_part_copy(x, i, q).start()
+
+    def x_other(i):
+        q = order[i]
+        x_arrival(1 - x, q).wait_recv()
+
+        @pl.when(c == duty[i])
         def _():
-            xbuf[s] = nbuf[i]
-
-    def tok_forward(q):
-        return remote(xbuf.at[q], xbuf.at[q], fwd_send.at[q], tok_recv.at[q], partner)
-
-    def tok_arrival(q):
-        return remote(xbuf.at[q], xbuf.at[q], fwd_send.at[q], tok_recv.at[q], partner)
+            x_part_copy(1 - x, i, q).start()
 
     re16 = dre_ref[pl.ds(g0, G), :]
     im16 = dim_ref[pl.ds(g0, G), :]
@@ -476,7 +586,6 @@
     lane = lax.broadcasted_iota(jnp.int32, (128, 16), 0)
     chan = lax.broadcasted_iota(jnp.int32, (128, 16), 1)
     steps = lax.broadcasted_iota(jnp.int32, (L, 128), 0).astype(jnp.float32) + 1.0
-    sel_hi = lax.broadcasted_iota(jnp.int32, (128, 16), 0)
 
     def table(g, carry):
         zr = coef[0, pl.ds(g, 1), :]
@@ -515,10 +624,90 @@
         )
         return carry
 
-    lax.fori_loop(0, G, table, 0)
-    for k in range(1, NS):
-        q = lax.rem(s + k, NS)
-        remote(shsend.at[q], shbuf.at[q], sh_send.at[q], sh_recv.at[q], {"sp": q}).wait_recv()
+    lax.fori_loop(0, G // 2, table, 0)
+    forward_all(0)
+    start_direct(1)
+    lax.fori_loop(G // 2, G, table, 0)
+    x_own(0)
+    x_own(1)
+    x_other(0)
+    for m in (2, 3):
+        load_w[m].wait()
+    forward_all(1)
+    w_own_y(2).start()
+    start_direct(2)
+
+    def weights(m):
+        return wbuf[m].reshape(KW, HC)
+
+    def y_copy(m, rows, i):
+        return remote(ysend.at[m, rows], yrecv.at[m, rows], y_send.at[m, i], y_recv.at[m, i], {"sp": s2})
+
+    def give_block(m, q, i):
+        rows = pl.ds(pl.multiple_of(q * L, L), L)
+        part = jnp.dot(xbuf[give, q], weights(m), preferred_element_type=jnp.float32)
+        ysend[m, rows] = part.astype(jnp.bfloat16)
+        y_copy(m, rows, q).start()
+
+    def give_all(m):
+        def one(i, carry):
+            rows = pl.ds(pl.multiple_of(i * 2 * L, 2 * L), 2 * L)
+            part = jnp.dot(
+                xbuf[give, pl.ds(2 * i, 2)].reshape(2 * L, KW), weights(m), preferred_element_type=jnp.float32
+            )
+            ysend[m, rows] = part.astype(jnp.bfloat16)
+            y_copy(m, rows, i).start()
+            return carry
+
+        lax.fori_loop(0, 2, one, 0)
+
+    def keep_all(m):
+        def one(i, carry):
+            rows = pl.ds(pl.multiple_of(i * 2 * L, 2 * L), 2 * L)
+            ykeep[m, rows] = jnp.dot(
+                xbuf[keep, pl.ds(2 * i, 2)].reshape(2 * L, KW), weights(m), preferred_element_type=jnp.float32
+            )
+            return carry
+
+        lax.fori_loop(0, 2, one, 0)
+
+    def finish(m):
+        for i in range(4 if m == 0 else 2):
+            size = SEQ // (4 if m == 0 else 2)
+            rows = pl.ds(i * size, size)
+            y_copy(m, rows, i).wait_recv()
+            fin[m, rows] = (ykeep[m, rows] + yrecv[m, rows].astype(jnp.float32)).astype(jnp.bfloat16)
+
+    own_w[0].wait()
+    wait_across(0)
+    for i in range(4):
+        if i >= 2:
+            x_own(i)
+
+        @pl.when(zh == 1)
+        def _():
+            give_block(0, order[i], i)
+
+        if i >= 1:
+            x_other(i)
+
+        @pl.when(zh == 0)
+        def _():
+            give_block(0, order[i], i)
+
+    own_w[1].wait()
+    wait_across(1)
+    give_all(1)
+    forward_all(2)
+    w_own_y(3).start()
+    start_direct(3)
+    keep_all(0)
+    keep_all(1)
+
+    for k in range(NS):
+        @pl.when(jnp.logical_not(jnp.logical_and(zh == 0, s == k)))
+        def _():
+            remote(shsend.at[k], shbuf.at[k], sh_send.at[k], sh_recv.at[k], {"sp": s1}).wait_recv()
     row_i = lax.broadcasted_iota(jnp.int32, (L, L), 0)
     col_i = lax.broadcasted_iota(jnp.int32, (L, L), 1)
     upper = (row_i <= col_i).astype(jnp.float32)
@@ -527,129 +716,9 @@
             shbuf[k], upper, precision=lax.Precision.HIGHEST, preferred_element_type=jnp.float32
         )
 
-    for k in range(NS):
-        q = lax.rem(s + k, NS)
-
-        @pl.when(c == owner)
-        def _():
-            @pl.when(q != s)
-            def _():
-                tok_arrival(q).wait_recv()
-
-            tok_forward(q).start()
-
-        @pl.when(c != owner)
-        def _():
-            tok_arrival(q).wait_recv()
-
-    def z_right(m, d):
-        return remote(pbuf.at[m, d], rbuf.at[0, m, d], z_send.at[m, d], zr_recv.at[m, d], {"sp": lax.rem(s + 1, NS)})
-
-    def z_left(m, d):
-        return remote(
-            pbuf.at[m, d], rbuf.at[1, m, d], z_send.at[m, d], zl_recv.at[m, d], {"sp": lax.rem(s + NS - 1, NS)}
-        )
-
-    def hop_right(m, k):
-        d = NS - 1 - k
-
-        @pl.when(d > s)
-        def _():
-            z_right(m, d).wait_recv()
-            pbuf[m, d] = (pbuf[m, d].astype(jnp.float32) + rbuf[0, m, d].astype(jnp.float32)).astype(jnp.bfloat16)
-            z_right(m, d).start()
-
-    def hop_left(m, d):
-        @pl.when(d < s)
-        def _():
-            z_left(m, d).wait_recv()
-            pbuf[m, d] = (pbuf[m, d].astype(jnp.float32) + rbuf[1, m, d].astype(jnp.float32)).astype(jnp.bfloat16)
-            z_left(m, d).start()
-
-    def each(hop, m):
-        def one(k, carry):
-            hop(m, k)
-            return carry
-
-        lax.fori_loop(0, NS, one, 0)
-
-    def relay(m):
-        @pl.when(jnp.logical_and(s > 0, s < NS // 2))
-        def _():
-            each(hop_right, m)
-            each(hop_left, m)
-
-        @pl.when(jnp.logical_and(s >= NS // 2, s < NS - 1))
-        def _():
-            each(hop_left, m)
-            each(hop_right, m)
-
-
-    def project(m, carry):
-        own_x(m).wait_recv()
-        own_y(m).wait_recv()
-        fwd_y(m).start()
-        fwd_x(m).start()
-
-        @pl.when(m < 2)
-        def _():
-            own_x(m + 2).start()
-            own_y(m + 2).start()
-
-        @pl.when(m > 0)
-        def _():
-            relay(m - 1)
-
-        diag_y = wbuf.at[m, fd, pl.ds(0, half)]
-        diag_x = wbuf.at[m, fd, pl.ds(half, half)]
-        remote(diag_y, diag_y, dy_send.at[m], dy_recv.at[m], {"fs": fy}).wait_recv()
-        remote(diag_x, diag_x, dx_send.at[m], dx_recv.at[m], {"fs": fx}).wait_recv()
-
-        def block(k, inner):
-            d = jnp.where(s < NS // 2, NS - 1 - k, k)
-            columns = pl.ds(pl.multiple_of(d * HC, HC), HC)
-            lhs = xbuf[...].reshape(SEQ, KW)
-            rhs = wbuf[m, :, :, columns].reshape(KW, HC)
-            part = jnp.dot(lhs, rhs, preferred_element_type=jnp.float32).astype(jnp.bfloat16)
-
-            pbuf[m, d] = part
-
-            @pl.when(jnp.logical_and(s == 0, d > 0))
-            def _():
-                z_right(m, d).start()
-
-            @pl.when(jnp.logical_and(s == NS - 1, d < NS - 1))
-            def _():
-                z_left(m, d).start()
-
-            return inner
-
-        return lax.fori_loop(0, NS, block, carry)
-
-    def finish(m):
-        @pl.when(s > 0)
-        def _():
-            z_right(m, s).wait_recv()
-
-        @pl.when(s < NS - 1)
-        def _():
-            z_left(m, s).wait_recv()
-
-        own = pbuf[m, s].astype(jnp.float32)
-
-        @pl.when(s == 0)
-        def _():
-            fin[m] = (own + rbuf[1, m, s].astype(jnp.float32)).astype(jnp.bfloat16)
-
-        @pl.when(s == NS - 1)
-        def _():
-            fin[m] = (own + rbuf[0, m, s].astype(jnp.float32)).astype(jnp.bfloat16)
-
-        @pl.when(jnp.logical_and(s > 0, s < NS - 1))
-        def _():
-            fin[m] = (own + rbuf[0, m, s].astype(jnp.float32) + rbuf[1, m, s].astype(jnp.float32)).astype(jnp.bfloat16)
-
-    lax.fori_loop(0, 3, project, 0)
+    own_w[2].wait()
+    wait_across(2)
+    give_all(2)
 
     finish(0)
     sign = jnp.where(lax.broadcasted_iota(jnp.int32, (8, 128), 1) < 64, -1.0, 1.0)
@@ -690,34 +759,53 @@
             return inner
 
         lax.fori_loop(0, 8, group, 0)
-        direct = skip_ref[:, pl.ds(pl.multiple_of(s * HC + b * 128, 128), 128)]
-        out = (yacc[...] + direct * u.astype(jnp.float32)).astype(jnp.bfloat16)
+        through = skip_ref[:, pl.ds(pl.multiple_of(hq * HC + b * 128, 128), 128)]
+        out = (yacc[...] + through * u.astype(jnp.float32)).astype(jnp.bfloat16)
         for k in range(NS):
             stb[k, :, lanes] = out[k * L : (k + 1) * L]
         return carry
 
-    lax.fori_loop(0, HC // 128, lane_block, 0)
-
-    lax.fori_loop(3, 4, project, 0)
-
-    def st_copy(d):
-        return remote(stb.at[d], sto.at[s], st_send.at[d], st_recv.at[s], {"sp": d})
-
-    def at_copy(d):
-        return remote(atb.at[d], ato.at[s], at_send.at[d], at_recv.at[s], {"sp": d})
-
-    def lt_copy(d):
-        return remote(ltb.at[d], lto.at[s], lt_send.at[d], lt_recv.at[s], {"sp": d})
-
-    for k in range(1, NS):
-        st_copy(lax.rem(s + k, NS)).start()
-    sto[s] = stb[s]
+    half_blocks = HC // 256
+    lax.fori_loop(0, half_blocks, lane_block, 0)
+    forward_all(3)
+    lax.fori_loop(half_blocks, HC // 128, lane_block, 0)
+    own_w[3].wait()
+    wait_across(3)
+    give_all(3)
+
+    def result_copy(src, dst, send, recv, d):
+        return remote(src.at[d], dst.at[hq], send.at[d], recv.at[hq], {"sp": d, "fs": home})
+
+    def result_arrival(src, dst, send, recv, h):
+        return remote(src.at[h], dst.at[h], send.at[h], recv.at[h], {"sp": s1})
+
+    def here(d):
+        return jnp.logical_and(zh == 0, s == d)
+
+    def send_results(src, dst, send, recv):
+        for d in range(NS):
+            @pl.when(jnp.logical_not(here(d)))
+            def _():
+                result_copy(src, dst, send, recv, d).start()
+
+        @pl.when(zh == 0)
+        def _():
+            dst[hq] = src[s]
+
+    def wait_results(src, dst, send, recv):
+        for h in range(NS):
+            @pl.when(jnp.logical_not(jnp.logical_and(zh == 0, hq == h)))
+            def _():
+                result_arrival(src, dst, send, recv, h).wait_recv()
+
+    send_results(stb, sto, st_send, st_recv)
+    keep_all(2)
+    keep_all(3)
 
     hd = HC // 2
-    relay(3)
     finish(1)
     finish(2)
-    lam = mix_ref[s]
+    lam = mix_ref[hq]
     totals = []
     for i in range(NS):
         width = (i + 1) * L
@@ -730,15 +818,13 @@
             allowed = kpos <= qpos
             sc = jnp.where(allowed, sc, -1e30)
             top = jnp.max(sc, axis=1, keepdims=True)
-            weights = jnp.where(allowed, jnp.exp(sc - top), 0.0)
-            total = jnp.sum(weights, axis=1, keepdims=True)
-            wts[m, i * L : (i + 1) * L, 0:width] = weights.astype(jnp.bfloat16)
+            weights_i = jnp.where(allowed, jnp.exp(sc - top), 0.0)
+            total = jnp.sum(weights_i, axis=1, keepdims=True)
+            wts[m, i * L : (i + 1) * L, 0:width] = weights_i.astype(jnp.bfloat16)
             totals.append(1.0 / total)
             logs = jnp.broadcast_to(top + jnp.log(total), (L, L)).T
             ltb[i, m : m + 1, :] = logs[0:1]
-    for k in range(1, NS):
-        lt_copy(lax.rem(s + k, NS)).start()
-    lto[s] = ltb[s]
+    send_results(ltb, lto, lt_send, lt_recv)
     finish(3)
     for i in range(NS):
         width = (i + 1) * L
@@ -753,16 +839,11 @@
         scale = lax.rsqrt(jnp.mean(raw * raw, axis=1, keepdims=True) + 1e-05)
         atb[i] = (raw * scale * hgain_ref[...]).astype(jnp.bfloat16)
 
-    for k in range(1, NS):
-        d = lax.rem(s + k, NS)
-        at_copy(d).start()
-    ato[s] = atb[s]
+    send_results(atb, ato, at_send, at_recv)
 
     for copy in big:
         copy.wait()
-    for k in range(1, NS):
-        q = lax.rem(s + k, NS)
-        remote(stb.at[q], sto.at[q], st_send.at[q], st_recv.at[q], {"sp": q}).wait_recv()
+    wait_results(stb, sto, st_send, st_recv)
     tiles = poutb.shape[0]
     width = D // tiles
     st_lhs = jnp.concatenate([sto[q] for q in range(NS)], axis=1)
@@ -773,9 +854,7 @@
         return carry
 
     lax.fori_loop(0, tiles, state_tile, 0)
-    for k in range(1, NS):
-        q = lax.rem(s + k, NS)
-        remote(atb.at[q], ato.at[q], at_send.at[q], at_recv.at[q], {"sp": q}).wait_recv()
+    wait_results(atb, ato, at_send, at_recv)
     at_lhs = jnp.concatenate([ato[q] for q in range(NS)], axis=1)
     rows = L // NT
     mine = pl.ds(pl.multiple_of(c * rows, rows), rows)
@@ -802,40 +881,59 @@
         return carry
 
     lax.fori_loop(0, tiles, last_tile, 0)
-    for k in range(1, NS):
-        q = lax.rem(s + k, NS)
-        remote(ltb.at[q], lto.at[q], lt_send.at[q], lt_recv.at[q], {"sp": q}).wait_recv()
+    wait_results(ltb, lto, lt_send, lt_recv)
     logt_ref[0] = lto[...]
 
     for m in range(4):
-        own_x(m).wait_send()
-        own_y(m).wait_send()
-        fwd_x(m).wait_send()
-        fwd_y(m).wait_send()
-        for k in range(1, NS):
-            z_right(m, lax.rem(s + k, NS)).wait_send()
-    for k in range(1, NS):
-        d = lax.rem(s + k, NS)
-        remote(shsend.at[d], shbuf.at[s], sh_send.at[d], sh_recv.at[s], {"sp": d}).wait_send()
-        st_copy(d).wait_send()
-        at_copy(d).wait_send()
-        lt_copy(d).wait_send()
-    for i in range(NB):
-        @pl.when(c * NB + i != s)
+        for j in range(3):
+            w_direct(m, j).wait_send()
+            w_forward(m, j).wait_send()
+        w_own_y(m).wait_send()
+        for i in range(4 if m == 0 else 2):
+            size = SEQ // (4 if m == 0 else 2)
+            y_copy(m, pl.ds(i * size, size), i).wait_send()
+
+    @pl.when(mine_half)
+    def _():
+        x_source(pair_target).wait_send()
+        x_cross_copy(0).wait_send()
+        x_part_copy(x, 0, s).wait_send()
+        x_part_copy(1 - x, 0, s).wait_send()
+
+    @pl.when(jnp.logical_not(mine_half))
+    def _():
+        x_source(far_target).wait_send()
+
+    for i in range(1, 4):
+        @pl.when(c == duty[i])
         def _():
-            tok_copy(i).wait_send()
-
-    @pl.when(c == owner)
-    def _():
-        for q in range(NS):
-            tok_forward(q).wait_send()
+            if i >= 2:
+                @pl.when(relays)
+                def _():
+                    x_relay_copy(i).wait_send()
+            x_cross_copy(i).wait_send()
+            x_part_copy(x, i, order[i]).wait_send()
+            x_part_copy(1 - x, i, order[i]).wait_send()
+
+    for xd in range(2):
+        for zd in range(2):
+            @pl.when(jnp.logical_not(to_self(xd, zd)))
+            def _():
+                shift_copy(xd, zd).wait_send()
+    for src, dst, send, recv in (
+        (stb, sto, st_send, st_recv), (atb, ato, at_send, at_recv), (ltb, lto, lt_send, lt_recv)
+    ):
+        for d in range(NS):
+            @pl.when(jnp.logical_not(here(d)))
+            def _():
+                result_copy(src, dst, send, recv, d).wait_send()
 
 
 def fused_device(sizes, *args):
     (tokens, norm_gain, ws, wq, wk, wv, dre, dim, logstep, shift, inre, inim, outre, outim, skip, mix, hgain, wos, woa) = args
     NS, NT, L, D, CW = sizes
-    KW, HC = (D // NS, CW // NS)
-    SEQ, G, NB, NF = (NS * L, HC // 16, NS // NT, 4)
+    KW, KB, HC = (D // 2, ws.shape[0], CW // NS)
+    SEQ, G = (NS * L, HC // 16)
     tiles = 8
     bf, f32 = (jnp.bfloat16, jnp.float32)
     V = pltpu.VMEM
@@ -846,11 +944,13 @@
     scratch = [
         V((L, 128), f32),
         V((L, 128), f32),
-        V((NB, L, KW), bf),
-        V((NS, L, KW), bf),
-        V((4, NF, ws.shape[0], CW), bf),
-        V((4, NS, SEQ, HC), bf),
-        V((2, 4, NS, SEQ, HC), bf),
+        V((L, KW), bf),
+        V((2, NS, L, KW), bf),
+        V((4, KB, CW), bf),
+        V((4, KW // KB, KB, HC), bf),
+        V((4, SEQ, HC), f32),
+        V((4, SEQ, HC), bf),
+        V((4, SEQ, HC), bf),
         V((4, SEQ, HC), bf),
         V((NS, G, L), f32),
         V((NS, G, L), f32),
@@ -876,13 +976,19 @@
         DMA((4,)),
         DMA((2,)),
         DMA((4,)),
+        DMA((4,)),
         DMA((2,)),
-        DMA((NB,)),
-        DMA((NS,)),
-        DMA((NS,)),
+        DMA,
+        DMA((2, 4)),
+        DMA((4,)),
+        DMA((2,)),
+        DMA((2, NS)),
+        DMA((4, 3)),
+        DMA((4, 4)),
+        DMA((4, 8)),
+        DMA((4, 4)),
+        DMA((4, 4)),
     ]
-    scratch += [DMA((4,))] * 8
-    scratch += [DMA((4, NS))] * 3
     scratch += [DMA((NS,))] * 8
     scratch += [DMA((tiles,))] * 2
     call = pl.pallas_call(
@@ -910,15 +1016,16 @@
     L, D = (tokens.shape[1], ws.shape[0] * sp * fs)
     CW = ws.shape[1]
     fits = (
-        fs == 4
+        sp == 4
+        and fs == 4
         and tp == 2
-        and sp % tp == 0
         and mix.shape[0] == sp
         and L == 128
         and CW == sp * 256
         and dre.shape == (sp * 16, 64)
         and inre.shape[2] == 16
-        and D % (sp * 128) == 0
+        and D == sp * 4 * ws.shape[0]
+        and ws.shape[0] % 128 == 0
     )
     if fits:
         return fused_device((sp, tp, L, D, CW), *args)

time: 137 us -> 126 us (0.920)
  Pallas kernels: 133 us -> 122 us
    pallas_call x1, Pallas kernels: 133 us -> 122 us  [fused_device(): call(tokens, norm_gain.reshape(1, -1), ws, wq, wk, wv, dre, dim, logstep,...]
where the time goes in v1:
time: 126 us; the launch traced here: 125 us
  Pallas kernels  122 us (97%)
  local copies, waits for them, and re-layouts  3.13 us (2%)
    pallas_call x1, Pallas kernels, fused_device(): call(tokens, norm_gain.reshape(1, -1), ws, wq, wk, wv, dre, dim, logstep,...  122 us
    unnamed x2, local copies, waits for them, and re-layouts  3.13 us

profile of v1, /device:TPU:1, one launch (start us, length us, event | category | flops | bytes accessed | tf_op | source)
XLA Modules:
  0.0 125.5 jit_solution(14554708602264944757)
XLA Ops:
  0.6 121.7 %shard_map.194 = (bf16[1,64,4096]{2,1,0:T(8,128)(2,1)}, f32[1,4,2,128]{3,2,1,0:T(2,128)}) custom-call(bf16[1,128,2048]{2,1,0:T(8,128)(2,1)} %tok_ref.1, f32[1,4096]{1,0:T(1,128)} %bitcast.7, bf16[256,1024]{1,0:T(8,128)(2,1)} %ws_ref.1, bf16[256,1024]{1,0:T(8,128)(2,1)} %wq_ref.1, bf16[256,1024]{1,0:T(8,128)(2,1)} %wk_ref.1, bf16[256,1024]{1,0:T(8,128)(2,1)} %wv_ref.1, ...), custom_call_target="tpu_custom_call" | custom-call | tf_op jit(solution)/shard_map/pallas_call | solution.py:1007
  122.3 1.9 %copy.23 = bf16[1,64,4096]{2,1,0:T(8,128)(2,1)} copy(bf16[1,64,4096]{2,1,0:T(8,128)(2,1)} %get-tuple-element.4) | data formatting | bytes 1048576
  124.2 1.3 %copy.24 = f32[1,4,2,128]{3,2,1,0:T(2,128)} copy(f32[1,4,2,128]{3,2,1,0:T(2,128)} %get-tuple-element.5) | data formatting | bytes 8192

commit v2 on v1

--- a/solution.py
+++ b/solution.py
@@ -509,66 +509,88 @@
     first_s = 2 - c
     near_core = jnp.where(s == first_s, c, 1 - c)
 
-    def x_source(where):
-        return remote(nbuf, xbuf.at[x, s], x_src, x_recv.at[x, s], where)
+    parts = x_src.shape[0]
+    strip = L // parts
+
+    def piece(n):
+        return pl.ds(n * strip, strip)
+
+    def x_copy(src, slot, q, n, send, where):
+        return remote(src, xbuf.at[slot, q, piece(n)], send, x_recv.at[slot, q, n], where)
 
     far_target = {"sp": near_s, "tp": near_core}
     pair_target = {"sp": s1, "tp": 1 - zh}
 
-    def x_part_copy(slot, i, q):
-        part = xbuf.at[slot, q]
-        return remote(part, part, x_part.at[slot, i], x_recv.at[slot, q], partner)
-
-    def x_cross_copy(i):
-        part = xbuf.at[x, order[i]]
-        return remote(part, part, x_cross.at[i], x_recv.at[x, order[i]], {"fs": fx})
-
-    def x_relay_copy(i):
-        part = xbuf.at[x, order[i]]
-        return remote(part, part, x_rel.at[i - 2], x_recv.at[x, order[i]], {"sp": s1})
-
-    def x_arrival(slot, q):
-        part = xbuf.at[slot, q]
-        return remote(part, part, x_src, x_recv.at[slot, q], partner)
+    def x_source(n, where):
+        return x_copy(nbuf.at[piece(n)], x, s, n, x_src.at[n], where)
+
+    def x_first(n):
+        return (
+            x_copy(nbuf.at[piece(n)], x, s, n, x_cross.at[0, n], {"fs": fx}),
+            x_copy(nbuf.at[piece(n)], x, s, n, x_part.at[x, 0, n], partner),
+        )
+
+    def x_pass(slot, i, n):
+        q = order[i]
+        part = xbuf.at[slot, q, piece(n)]
+        return x_copy(part, slot, q, n, x_part.at[slot, i, n], partner)
+
+    def x_cross_copy(i, n):
+        q = order[i]
+        return x_copy(xbuf.at[x, q, piece(n)], x, q, n, x_cross.at[i, n], {"fs": fx})
+
+    def x_relay_copy(i, n):
+        q = order[i]
+        return x_copy(xbuf.at[x, q, piece(n)], x, q, n, x_rel.at[i - 2, n], {"sp": s1})
+
+    def x_wait(slot, q, n):
+        x_copy(xbuf.at[slot, q, piece(n)], slot, q, n, x_src.at[n], partner).wait_recv()
 
     relays = zl == 1 - zh
 
     @pl.when(mine_half)
     def _():
         xbuf[x, s] = nbuf[...]
-        x_source(pair_target).start()
-        remote(nbuf, xbuf.at[x, s], x_cross.at[0], x_recv.at[x, s], {"fs": fx}).start()
-        remote(nbuf, xbuf.at[x, s], x_part.at[x, 0], x_recv.at[x, s], partner).start()
+        for n in range(parts):
+            x_source(n, pair_target).start()
+            for copy in x_first(n):
+                copy.start()
 
     @pl.when(jnp.logical_not(mine_half))
     def _():
-        x_source(far_target).start()
+        for n in range(parts):
+            x_source(n, far_target).start()
 
     def x_own(i):
-        q = order[i]
-        if i == 0:
-            @pl.when(jnp.logical_not(mine_half))
-            def _():
-                x_arrival(x, q).wait_recv()
-            return
-        x_arrival(x, q).wait_recv()
-
         @pl.when(c == duty[i])
         def _():
-            if i >= 2:
-                @pl.when(relays)
-                def _():
-                    x_relay_copy(i).start()
-            x_cross_copy(i).start()
-            x_part_copy(x, i, q).start()
+            for n in range(parts):
+                x_wait(x, order[i], n)
+                if i >= 2:
+                    @pl.when(relays)
+                    def _():
+                        x_relay_copy(i, n).start()
+                x_cross_copy(i, n).start()
+                x_pass(x, i, n).start()
 
     def x_other(i):
-        q = order[i]
-        x_arrival(1 - x, q).wait_recv()
-
         @pl.when(c == duty[i])
         def _():
-            x_part_copy(1 - x, i, q).start()
+            for n in range(parts):
+                x_wait(1 - x, order[i], n)
+                x_pass(1 - x, i, n).start()
+
+    def x_need(i):
+        @pl.when(c != duty[i])
+        def _():
+            for n in range(parts):
+                x_wait(x, order[i], n)
+
+    def x_need_other(i):
+        @pl.when(c != duty[i])
+        def _():
+            for n in range(parts):
+                x_wait(1 - x, order[i], n)
 
     re16 = dre_ref[pl.ds(g0, G), :]
     im16 = dim_ref[pl.ds(g0, G), :]
@@ -626,16 +648,16 @@
 
     lax.fori_loop(0, G // 2, table, 0)
     forward_all(0)
-    start_direct(1)
-    lax.fori_loop(G // 2, G, table, 0)
-    x_own(0)
-    x_own(1)
-    x_other(0)
     for m in (2, 3):
         load_w[m].wait()
-    forward_all(1)
-    w_own_y(2).start()
-    start_direct(2)
+        w_own_y(m).start()
+    lax.fori_loop(G // 2, G, table, 0)
+    x_own(1)
+    x_own(2)
+    x_own(3)
+    start_direct(1)
+    x_other(0)
+    x_other(1)
 
     def weights(m):
         return wbuf[m].reshape(KW, HC)
@@ -680,26 +702,26 @@
 
     own_w[0].wait()
     wait_across(0)
-    for i in range(4):
-        if i >= 2:
-            x_own(i)
-
-        @pl.when(zh == 1)
-        def _():
-            give_block(0, order[i], i)
-
-        if i >= 1:
-            x_other(i)
-
-        @pl.when(zh == 0)
-        def _():
-            give_block(0, order[i], i)
-
+    x_need(0)
+    x_need(1)
+    x_need_other(0)
+    x_need_other(1)
+    give_block(0, order[0], 0)
+    give_block(0, order[1], 1)
+    x_other(2)
+    x_other(3)
+    forward_all(1)
+    start_direct(2)
+    x_need(2)
+    x_need(3)
+    x_need_other(2)
+    x_need_other(3)
+    give_block(0, order[2], 2)
+    give_block(0, order[3], 3)
     own_w[1].wait()
     wait_across(1)
     give_all(1)
     forward_all(2)
-    w_own_y(3).start()
     start_direct(3)
     keep_all(0)
     keep_all(1)
@@ -895,25 +917,28 @@
 
     @pl.when(mine_half)
     def _():
-        x_source(pair_target).wait_send()
-        x_cross_copy(0).wait_send()
-        x_part_copy(x, 0, s).wait_send()
-        x_part_copy(1 - x, 0, s).wait_send()
+        for n in range(parts):
+            x_source(n, pair_target).wait_send()
+            for copy in x_first(n):
+                copy.wait_send()
+            x_pass(1 - x, 0, n).wait_send()
 
     @pl.when(jnp.logical_not(mine_half))
     def _():
-        x_source(far_target).wait_send()
+        for n in range(parts):
+            x_source(n, far_target).wait_send()
 
     for i in range(1, 4):
         @pl.when(c == duty[i])
         def _():
-            if i >= 2:
-                @pl.when(relays)
-                def _():
-                    x_relay_copy(i).wait_send()
-            x_cross_copy(i).wait_send()
-            x_part_copy(x, i, order[i]).wait_send()
-            x_part_copy(1 - x, i, order[i]).wait_send()
+            for n in range(parts):
+                if i >= 2:
+                    @pl.when(relays)
+                    def _():
+                        x_relay_copy(i, n).wait_send()
+                x_cross_copy(i, n).wait_send()
+                x_pass(x, i, n).wait_send()
+                x_pass(1 - x, i, n).wait_send()
 
     for xd in range(2):
         for zd in range(2):
@@ -934,7 +959,7 @@
     NS, NT, L, D, CW = sizes
     KW, KB, HC = (D // 2, ws.shape[0], CW // NS)
     SEQ, G = (NS * L, HC // 16)
-    tiles = 8
+    tiles, pieces = (8, 2)
     bf, f32 = (jnp.bfloat16, jnp.float32)
     V = pltpu.VMEM
     DMA = pltpu.SemaphoreType.DMA
@@ -978,11 +1003,11 @@
         DMA((4,)),
         DMA((4,)),
         DMA((2,)),
-        DMA,
-        DMA((2, 4)),
-        DMA((4,)),
-        DMA((2,)),
-        DMA((2, NS)),
+        DMA((pieces,)),
+        DMA((2, 4, pieces)),
+        DMA((4, pieces)),
+        DMA((2, pieces)),
+        DMA((2, NS, pieces)),
         DMA((4, 3)),
         DMA((4, 4)),
         DMA((4, 8)),

time: 126 us -> 109 us (0.87)
  Pallas kernels: 122 us -> 105 us
    pallas_call x1, Pallas kernels: 122 us -> 105 us  [fused_device(): call(tokens, norm_gain.reshape(1, -1), ws, wq, wk, wv, dre, dim, logstep,...]
where the time goes in v2:
time: 109 us
  Pallas kernels  105 us (96%)
  local copies, waits for them, and re-layouts  3.13 us (3%)
    pallas_call x1, Pallas kernels, fused_device(): call(tokens, norm_gain.reshape(1, -1), ws, wq, wk, wv, dre, dim, logstep,...  105 us
    unnamed x2, local copies, waits for them, and re-layouts  3.13 us

profile of v2, /device:TPU:1, one launch (start us, length us, event | category | flops | bytes accessed | tf_op | source)
XLA Modules:
  0.0 108.9 jit_solution(6828028491038002156)
XLA Ops:
  0.6 105.1 %shard_map.194 = (bf16[1,64,4096]{2,1,0:T(8,128)(2,1)}, f32[1,4,2,128]{3,2,1,0:T(2,128)}) custom-call(bf16[1,128,2048]{2,1,0:T(8,128)(2,1)} %tok_ref.1, f32[1,4096]{1,0:T(1,128)} %bitcast.7, bf16[256,1024]{1,0:T(8,128)(2,1)} %ws_ref.1, bf16[256,1024]{1,0:T(8,128)(2,1)} %wq_ref.1, bf16[256,1024]{1,0:T(8,128)(2,1)} %wk_ref.1, bf16[256,1024]{1,0:T(8,128)(2,1)} %wv_ref.1, ...), custom_call_target="tpu_custom_call" | custom-call | tf_op jit(solution)/shard_map/pallas_call | solution.py:1032
  105.7 1.9 %copy.23 = bf16[1,64,4096]{2,1,0:T(8,128)(2,1)} copy(bf16[1,64,4096]{2,1,0:T(8,128)(2,1)} %get-tuple-element.4) | data formatting | bytes 1048576
  107.6 1.3 %copy.24 = f32[1,4,2,128]{3,2,1,0:T(2,128)} copy(f32[1,4,2,128]{3,2,1,0:T(2,128)} %get-tuple-element.5) | data formatting | bytes 8192

commit v3 on v2

--- a/solution.py
+++ b/solution.py
@@ -322,18 +322,16 @@
     acc,
     poutb,
     precb,
+    obuf,
+    o_sem,
     loc_sem,
     wo_sem,
     w_loc,
     w_own,
     stat_sem,
-    x_src,
-    x_part,
-    x_cross,
-    x_rel,
+    x_send,
     x_recv,
-    wd_send,
-    wy_send,
+    w_send,
     w_recv,
     y_send,
     y_recv,
@@ -375,6 +373,21 @@
             src_ref=src, dst_ref=dst, send_sem=send, recv_sem=recv, device_id=where, device_id_type=MESH
         )
 
+    def drain_send(part, sem):
+        remote(part, part, sem, stat_sem.at[1], partner).wait_send()
+
+    def drain_recv(part, sem):
+        remote(part, part, stat_sem.at[0], sem, partner).wait_recv()
+
+    def drain_four(drain, ref, sem):
+        @pl.when(zh == 0)
+        def _():
+            drain(ref.at[0 : NS - 1], sem)
+
+        @pl.when(zh == 1)
+        def _():
+            drain(ref, sem)
+
     g0 = pl.multiple_of(hq * G, G)
     kbo = zl * 4 + f
 
@@ -434,26 +447,16 @@
         ((1 - x) * 2 + 1 - zl, {"sp": s1, "fs": fx}),
     )
     arrive = (zl * 4 + fx, (1 - zl) * 4 + f, (1 - zl) * 4 + fx)
-    across = (zl * 4 + fy, zl * 4 + fd, (1 - zl) * 4 + fy, (1 - zl) * 4 + fd)
-
     def w_direct(m, j):
         h, where = direct[j]
-        return remote(
-            wl.at[m, :, head_columns(h)], wbuf.at[m, kbo], wd_send.at[m, j], w_recv.at[m, kbo], where
-        )
+        return remote(wl.at[m, :, head_columns(h)], wbuf.at[m, kbo], w_send, w_recv.at[m, j], where)
 
     def w_own_y(m):
-        return remote(
-            wl.at[m, :, head_columns(hq)], wbuf.at[m, kbo], wy_send.at[m, 3], w_recv.at[m, kbo], {"fs": fy}
-        )
+        return remote(wl.at[m, :, head_columns(hq)], wbuf.at[m, kbo], w_send, w_recv.at[m, 3], {"fs": fy})
 
     def w_forward(m, j):
         part = wbuf.at[m, arrive[j]]
-        return remote(part, part, wy_send.at[m, j], w_recv.at[m, arrive[j]], {"fs": fy})
-
-    def w_arrival(m, kb):
-        part = wbuf.at[m, kb]
-        return remote(part, part, wy_send.at[m, 0], w_recv.at[m, kb], {"fs": fy})
+        return remote(part, part, w_send, w_recv.at[m, 3], {"fs": fy})
 
     def start_direct(m):
         for j in (2, 1, 0):
@@ -461,12 +464,11 @@
 
     def forward_all(m):
         for j in range(3):
-            w_arrival(m, arrive[j]).wait_recv()
+            drain_recv(wbuf.at[m, arrive[j]], w_recv.at[m, j])
             w_forward(m, j).start()
 
     def wait_across(m):
-        for kb in across:
-            w_arrival(m, kb).wait_recv()
+        drain_recv(wbuf.at[m, 0:4], w_recv.at[m, 3])
 
     load_w[0].wait()
     start_direct(0)
@@ -478,7 +480,7 @@
         zhd = xd + x - 2 * xd * x
         h = 2 * xd + zd
         return remote(
-            shsend.at[h], shbuf.at[s], sh_send.at[h], sh_recv.at[s], {"sp": 2 * zhd + zd, "fs": 2 * y + xd}
+            shsend.at[h], shbuf.at[s], sh_send, sh_recv, {"sp": 2 * zhd + zd, "fs": 2 * y + xd}
         )
 
     def to_self(xd, zd):
@@ -509,52 +511,36 @@
     first_s = 2 - c
     near_core = jnp.where(s == first_s, c, 1 - c)
 
-    parts = x_src.shape[0]
+    parts = x_recv.shape[2]
     strip = L // parts
 
     def piece(n):
         return pl.ds(n * strip, strip)
 
-    def x_copy(src, slot, q, n, send, where):
-        return remote(src, xbuf.at[slot, q, piece(n)], send, x_recv.at[slot, q, n], where)
+    def x_copy(src, slot, q, n, where):
+        return remote(src, xbuf.at[4 * slot + q, piece(n)], x_send, x_recv.at[slot, q, n], where)
 
     far_target = {"sp": near_s, "tp": near_core}
     pair_target = {"sp": s1, "tp": 1 - zh}
 
     def x_source(n, where):
-        return x_copy(nbuf.at[piece(n)], x, s, n, x_src.at[n], where)
-
-    def x_first(n):
-        return (
-            x_copy(nbuf.at[piece(n)], x, s, n, x_cross.at[0, n], {"fs": fx}),
-            x_copy(nbuf.at[piece(n)], x, s, n, x_part.at[x, 0, n], partner),
-        )
-
-    def x_pass(slot, i, n):
+        return x_copy(nbuf.at[piece(n)], x, s, n, where)
+
+    def x_step(slot, i, n, where):
         q = order[i]
-        part = xbuf.at[slot, q, piece(n)]
-        return x_copy(part, slot, q, n, x_part.at[slot, i, n], partner)
-
-    def x_cross_copy(i, n):
-        q = order[i]
-        return x_copy(xbuf.at[x, q, piece(n)], x, q, n, x_cross.at[i, n], {"fs": fx})
-
-    def x_relay_copy(i, n):
-        q = order[i]
-        return x_copy(xbuf.at[x, q, piece(n)], x, q, n, x_rel.at[i - 2, n], {"sp": s1})
+        return x_copy(xbuf.at[4 * slot + q, piece(n)], slot, q, n, where)
 
     def x_wait(slot, q, n):
-        x_copy(xbuf.at[slot, q, piece(n)], slot, q, n, x_src.at[n], partner).wait_recv()
+        drain_recv(xbuf.at[4 * slot + q, piece(n)], x_recv.at[slot, q, n])
 
     relays = zl == 1 - zh
 
     @pl.when(mine_half)
     def _():
-        xbuf[x, s] = nbuf[...]
+        xbuf[4 * x + s] = nbuf[...]
         for n in range(parts):
-            x_source(n, pair_target).start()
-            for copy in x_first(n):
-                copy.start()
+            for where in (pair_target, {"fs": fx}, partner):
+                x_source(n, where).start()
 
     @pl.when(jnp.logical_not(mine_half))
     def _():
@@ -569,16 +555,16 @@
                 if i >= 2:
                     @pl.when(relays)
                     def _():
-                        x_relay_copy(i, n).start()
-                x_cross_copy(i, n).start()
-                x_pass(x, i, n).start()
+                        x_step(x, i, n, {"sp": s1}).start()
+                x_step(x, i, n, {"fs": fx}).start()
+                x_step(x, i, n, partner).start()
 
     def x_other(i):
         @pl.when(c == duty[i])
         def _():
             for n in range(parts):
                 x_wait(1 - x, order[i], n)
-                x_pass(1 - x, i, n).start()
+                x_step(1 - x, i, n, partner).start()
 
     def x_need(i):
         @pl.when(c != duty[i])
@@ -663,11 +649,11 @@
         return wbuf[m].reshape(KW, HC)
 
     def y_copy(m, rows, i):
-        return remote(ysend.at[m, rows], yrecv.at[m, rows], y_send.at[m, i], y_recv.at[m, i], {"sp": s2})
+        return remote(ysend.at[m, rows], yrecv.at[m, rows], y_send, y_recv.at[m], {"sp": s2})
 
     def give_block(m, q, i):
         rows = pl.ds(pl.multiple_of(q * L, L), L)
-        part = jnp.dot(xbuf[give, q], weights(m), preferred_element_type=jnp.float32)
+        part = jnp.dot(xbuf[4 * give + q], weights(m), preferred_element_type=jnp.float32)
         ysend[m, rows] = part.astype(jnp.bfloat16)
         y_copy(m, rows, q).start()
 
@@ -675,7 +661,7 @@
         def one(i, carry):
             rows = pl.ds(pl.multiple_of(i * 2 * L, 2 * L), 2 * L)
             part = jnp.dot(
-                xbuf[give, pl.ds(2 * i, 2)].reshape(2 * L, KW), weights(m), preferred_element_type=jnp.float32
+                xbuf[pl.ds(4 * give + 2 * i, 2)].reshape(2 * L, KW), weights(m), preferred_element_type=jnp.float32
             )
             ysend[m, rows] = part.astype(jnp.bfloat16)
             y_copy(m, rows, i).start()
@@ -687,18 +673,15 @@
         def one(i, carry):
             rows = pl.ds(pl.multiple_of(i * 2 * L, 2 * L), 2 * L)
             ykeep[m, rows] = jnp.dot(
-                xbuf[keep, pl.ds(2 * i, 2)].reshape(2 * L, KW), weights(m), preferred_element_type=jnp.float32
+                xbuf[pl.ds(4 * keep + 2 * i, 2)].reshape(2 * L, KW), weights(m), preferred_element_type=jnp.float32
             )
             return carry
 
         lax.fori_loop(0, 2, one, 0)
 
     def finish(m):
-        for i in range(4 if m == 0 else 2):
-            size = SEQ // (4 if m == 0 else 2)
-            rows = pl.ds(i * size, size)
-            y_copy(m, rows, i).wait_recv()
-            fin[m, rows] = (ykeep[m, rows] + yrecv[m, rows].astype(jnp.float32)).astype(jnp.bfloat16)
+        drain_recv(yrecv.at[m], y_recv.at[m])
+        fin[m] = (ykeep[m] + yrecv[m].astype(jnp.float32)).astype(jnp.bfloat16)
 
     own_w[0].wait()
     wait_across(0)
@@ -708,9 +691,9 @@
     x_need_other(1)
     give_block(0, order[0], 0)
     give_block(0, order[1], 1)
+    forward_all(1)
     x_other(2)
     x_other(3)
-    forward_all(1)
     start_direct(2)
     x_need(2)
     x_need(3)
@@ -726,10 +709,7 @@
     keep_all(0)
     keep_all(1)
 
-    for k in range(NS):
-        @pl.when(jnp.logical_not(jnp.logical_and(zh == 0, s == k)))
-        def _():
-            remote(shsend.at[k], shbuf.at[k], sh_send.at[k], sh_recv.at[k], {"sp": s1}).wait_recv()
+    drain_four(drain_recv, shbuf, sh_recv)
     row_i = lax.broadcasted_iota(jnp.int32, (L, L), 0)
     col_i = lax.broadcasted_iota(jnp.int32, (L, L), 1)
     upper = (row_i <= col_i).astype(jnp.float32)
@@ -796,10 +776,7 @@
     give_all(3)
 
     def result_copy(src, dst, send, recv, d):
-        return remote(src.at[d], dst.at[hq], send.at[d], recv.at[hq], {"sp": d, "fs": home})
-
-    def result_arrival(src, dst, send, recv, h):
-        return remote(src.at[h], dst.at[h], send.at[h], recv.at[h], {"sp": s1})
+        return remote(src.at[d], dst.at[hq], send, recv, {"sp": d, "fs": home})
 
     def here(d):
         return jnp.logical_and(zh == 0, s == d)
@@ -814,11 +791,8 @@
         def _():
             dst[hq] = src[s]
 
-    def wait_results(src, dst, send, recv):
-        for h in range(NS):
-            @pl.when(jnp.logical_not(jnp.logical_and(zh == 0, hq == h)))
-            def _():
-                result_arrival(src, dst, send, recv, h).wait_recv()
+    def wait_results(dst, recv):
+        drain_four(drain_recv, dst, recv)
 
     send_results(stb, sto, st_send, st_recv)
     keep_all(2)
@@ -865,93 +839,69 @@
 
     for copy in big:
         copy.wait()
-    wait_results(stb, sto, st_send, st_recv)
     tiles = poutb.shape[0]
     width = D // tiles
-    st_lhs = jnp.concatenate([sto[q] for q in range(NS)], axis=1)
+    def term(src, i, columns):
+        lhs = jnp.concatenate([src[h] for h in range(NS)], axis=1)
+        return jnp.dot(lhs, wo[i, :, columns], preferred_element_type=jnp.float32)
+
+    def tile_columns(n):
+        return pl.ds(pl.multiple_of(n * width, width), width)
 
     def state_tile(n, carry):
-        columns = pl.ds(pl.multiple_of(n * width, width), width)
-        acc[:, columns] = jnp.dot(st_lhs, wo[0, :, columns], preferred_element_type=jnp.float32)
+        acc[:, tile_columns(n)] = term(sto, 0, tile_columns(n))
         return carry
 
+    wait_results(sto, st_recv)
     lax.fori_loop(0, tiles, state_tile, 0)
-    wait_results(atb, ato, at_send, at_recv)
-    at_lhs = jnp.concatenate([ato[q] for q in range(NS)], axis=1)
+    wait_results(lto, lt_recv)
+    logs_out = pltpu.make_async_copy(lto, logt_ref.at[0], o_sem.at[tiles])
+    logs_out.start()
+    drain_send(wbuf.at[:, 0:7], w_send)
+    drain_send(ysend, y_send)
+
+    @pl.when(relays)
+    def _():
+        drain_send(xbuf, x_send)
+
+    @pl.when(jnp.logical_not(relays))
+    def _():
+        drain_send(xbuf.at[0:7], x_send)
+
+    drain_four(drain_send, shsend, sh_send)
+    drain_four(drain_send, stb, st_send)
+    wait_results(ato, at_recv)
     rows = L // NT
     mine = pl.ds(pl.multiple_of(c * rows, rows), rows)
 
     def p_copy(n):
         theirs = pl.ds(pl.multiple_of((1 - c) * rows, rows), rows)
-        return remote(poutb.at[n, theirs], precb.at[n], p_send.at[n], p_recv.at[n], partner)
+        return remote(poutb.at[n, theirs], precb.at[n], p_send, p_recv.at[n], partner)
 
     def attn_tile(n, carry):
-        columns = pl.ds(pl.multiple_of(n * width, width), width)
-        part = acc[:, columns] + jnp.dot(at_lhs, wo[1, :, columns], preferred_element_type=jnp.float32)
+        part = acc[:, tile_columns(n)] + term(ato, 1, tile_columns(n))
         poutb[n] = part.astype(jnp.bfloat16)
         p_copy(n).start()
         return carry
 
     lax.fori_loop(0, tiles, attn_tile, 0)
 
+    def out_copy(n):
+        return pltpu.make_async_copy(obuf.at[n], mixed_ref.at[0, :, tile_columns(n)], o_sem.at[n])
+
     def last_tile(n, carry):
-        columns = pl.ds(pl.multiple_of(n * width, width), width)
-        p_copy(n).wait()
-        mixed_ref[0, :, columns] = (
-            poutb[n, mine, :].astype(jnp.float32) + precb[n].astype(jnp.float32)
-        ).astype(jnp.bfloat16)
+        p_copy(n).wait_recv()
+        obuf[n] = (poutb[n, mine, :].astype(jnp.float32) + precb[n].astype(jnp.float32)).astype(jnp.bfloat16)
+        out_copy(n).start()
         return carry
 
     lax.fori_loop(0, tiles, last_tile, 0)
-    wait_results(ltb, lto, lt_send, lt_recv)
-    logt_ref[0] = lto[...]
-
-    for m in range(4):
-        for j in range(3):
-            w_direct(m, j).wait_send()
-            w_forward(m, j).wait_send()
-        w_own_y(m).wait_send()
-        for i in range(4 if m == 0 else 2):
-            size = SEQ // (4 if m == 0 else 2)
-            y_copy(m, pl.ds(i * size, size), i).wait_send()
-
-    @pl.when(mine_half)
-    def _():
-        for n in range(parts):
-            x_source(n, pair_target).wait_send()
-            for copy in x_first(n):
-                copy.wait_send()
-            x_pass(1 - x, 0, n).wait_send()
-
-    @pl.when(jnp.logical_not(mine_half))
-    def _():
-        for n in range(parts):
-            x_source(n, far_target).wait_send()
-
-    for i in range(1, 4):
-        @pl.when(c == duty[i])
-        def _():
-            for n in range(parts):
-                if i >= 2:
-                    @pl.when(relays)
-                    def _():
-                        x_relay_copy(i, n).wait_send()
-                x_cross_copy(i, n).wait_send()
-                x_pass(x, i, n).wait_send()
-                x_pass(1 - x, i, n).wait_send()
-
-    for xd in range(2):
-        for zd in range(2):
-            @pl.when(jnp.logical_not(to_self(xd, zd)))
-            def _():
-                shift_copy(xd, zd).wait_send()
-    for src, dst, send, recv in (
-        (stb, sto, st_send, st_recv), (atb, ato, at_send, at_recv), (ltb, lto, lt_send, lt_recv)
-    ):
-        for d in range(NS):
-            @pl.when(jnp.logical_not(here(d)))
-            def _():
-                result_copy(src, dst, send, recv, d).wait_send()
+    for n in range(tiles):
+        out_copy(n).wait()
+    logs_out.wait()
+    drain_send(precb, p_send)
+    drain_four(drain_send, atb, at_send)
+    drain_four(drain_send, ltb, lt_send)
 
 
 def fused_device(sizes, *args):
@@ -959,7 +909,7 @@
     NS, NT, L, D, CW = sizes
     KW, KB, HC = (D // 2, ws.shape[0], CW // NS)
     SEQ, G = (NS * L, HC // 16)
-    tiles, pieces = (8, 2)
+    tiles, pieces = (4, 2)
     bf, f32 = (jnp.bfloat16, jnp.float32)
     V = pltpu.VMEM
     DMA = pltpu.SemaphoreType.DMA
@@ -970,7 +920,7 @@
         V((L, 128), f32),
         V((L, 128), f32),
         V((L, KW), bf),
-        V((2, NS, L, KW), bf),
+        V((2 * NS, L, KW), bf),
         V((4, KB, CW), bf),
         V((4, KW // KB, KB, HC), bf),
         V((4, SEQ, HC), f32),
@@ -998,24 +948,22 @@
         V((L, D), f32),
         V((tiles, L, D // tiles), bf),
         V((tiles, L // NT, D // tiles), bf),
+        V((tiles, L // NT, D // tiles), bf),
+        DMA((tiles + 1,)),
         DMA((4,)),
         DMA((2,)),
         DMA((4,)),
         DMA((4,)),
         DMA((2,)),
-        DMA((pieces,)),
-        DMA((2, 4, pieces)),
-        DMA((4, pieces)),
-        DMA((2, pieces)),
+        DMA,
         DMA((2, NS, pieces)),
-        DMA((4, 3)),
+        DMA,
         DMA((4, 4)),
-        DMA((4, 8)),
-        DMA((4, 4)),
-        DMA((4, 4)),
+        DMA,
+        DMA((4,)),
     ]
-    scratch += [DMA((NS,))] * 8
-    scratch += [DMA((tiles,))] * 2
+    scratch += [DMA] * 9
+    scratch += [DMA((tiles,))]
     call = pl.pallas_call(
         functools.partial(fused_kernel, sizes),
         out_shape=(
@@ -1023,17 +971,44 @@
             jax.ShapeDtypeStruct((1, NS, 2, L), f32),
         ),
         in_specs=[vmem, vmem, hbm, hbm, hbm, hbm, vmem, vmem, smem, vmem, hbm, hbm, hbm, hbm, vmem, smem, vmem, hbm, hbm],
-        out_specs=(vmem, vmem),
+        out_specs=(hbm, hbm),
         scratch_shapes=scratch,
         compiler_params=pltpu.CompilerParams(
             collective_id=0, has_side_effects=True, vmem_limit_bytes=67043328
         ),
     )
-    return call(
+    mixed, logs = call(
         tokens, norm_gain.reshape(1, -1), ws, wq, wk, wv, dre, dim, logstep, shift,
         inre.transpose(0, 2, 1), inim.transpose(0, 2, 1), outre, outim,
         skip.reshape(1, -1), mix, hgain.reshape(1, -1), wos, woa,
     )
+    return pl.pallas_call(
+        hand_over,
+        out_shape=(
+            jax.ShapeDtypeStruct(mixed.shape, mixed.dtype),
+            jax.ShapeDtypeStruct(logs.shape, logs.dtype),
+        ),
+        in_specs=[hbm, hbm],
+        out_specs=(hbm, hbm),
+        scratch_shapes=[V(mixed.shape, bf), V(logs.shape, f32), DMA((5,)), DMA((5,))],
+    )(mixed, logs)
+
+
+def hand_over(mixed_ref, logs_ref, mixed_out, logs_out, mixed_buf, logs_buf, in_sem, out_sem):
+    rows = mixed_buf.shape[1] // 4
+    views = [
+        tuple(ref.at[:, pl.ds(i * rows, rows)] for ref in (mixed_ref, mixed_buf, mixed_out)) for i in range(4)
+    ]
+    views.append((logs_ref, logs_buf, logs_out))
+    loads = [pltpu.make_async_copy(v[0], v[1], in_sem.at[i]) for i, v in enumerate(views)]
+    stores = [pltpu.make_async_copy(v[1], v[2], out_sem.at[i]) for i, v in enumerate(views)]
+    for copy in loads:
+        copy.start()
+    for load, store in zip(loads, stores):
+        load.wait()
+        store.start()
+    for copy in stores:
+        copy.wait()
 
 
 def choose_device(sp, fs, tp, *args):

time: 109 us -> 106 us (0.972)
  local copies, waits for them, and re-layouts: 3.13 us -> 0 us
    unnamed x2 -> x0, local copies, waits for them, and re-layouts: 3.13 us -> none
    pallas_call x1, Pallas kernels: 105 us -> 103 us  [fused_device(): call(tokens, norm_gain.reshape(1, -1), ws, wq, wk, wv, dre, dim, logstep,...]
    pallas_call x0 -> x1, Pallas kernels: none -> 1.84 us  [fused_device(): pl.pallas_call(hand_over, out_shape=(jax.ShapeDtypeStruct(mixed.shape, mi...]
where the time goes in v3:
time: 106 us
  Pallas kernels  105 us (99%)
    pallas_call x1, Pallas kernels, fused_device(): call(tokens, norm_gain.reshape(1, -1), ws, wq, wk, wv, dre, dim, logstep,...  103 us

profile of v3, /device:TPU:1, one launch (start us, length us, event | category | flops | bytes accessed | tf_op | source)
XLA Modules:
  0.0 105.6 jit_solution(6193826964116407471)
XLA Ops:
  0.6 103.1 %shard_map.194 = (bf16[1,64,4096]{2,1,0:T(8,128)(2,1)}, f32[1,4,2,128]{3,2,1,0:T(2,128)}) custom-call(bf16[1,128,2048]{2,1,0:T(8,128)(2,1)} %tok_ref.1, f32[1,4096]{1,0:T(1,128)} %bitcast.7, bf16[256,1024]{1,0:T(8,128)(2,1)} %ws_ref.1, bf16[256,1024]{1,0:T(8,128)(2,1)} %wq_ref.1, bf16[256,1024]{1,0:T(8,128)(2,1)} %wk_ref.1, bf16[256,1024]{1,0:T(8,128)(2,1)} %wv_ref.1, ...), custom_call_target="tpu_custom_call" | custom-call | tf_op jit(solution)/shard_map/pallas_call | solution.py:980
  103.8 1.8 %shard_map.195 = (bf16[1,64,4096]{2,1,0:T(8,128)(2,1)}, f32[1,4,2,128]{3,2,1,0:T(2,128)}) custom-call(bf16[1,64,4096]{2,1,0:T(8,128)(2,1)} %get-tuple-element.4.mixed_ref, f32[1,4,2,128]{3,2,1,0:T(2,128)} %get-tuple-element.5.logs_ref), custom_call_target="tpu_custom_call" | custom-call | tf_op jit(solution)/shard_map/pallas_call | solution.py:985

commit v4 on v3

--- a/solution.py
+++ b/solution.py
@@ -692,9 +692,9 @@
     give_block(0, order[0], 0)
     give_block(0, order[1], 1)
     forward_all(1)
+    start_direct(2)
     x_other(2)
     x_other(3)
-    start_direct(2)
     x_need(2)
     x_need(3)
     x_need_other(2)
@@ -782,7 +782,7 @@
         return jnp.logical_and(zh == 0, s == d)
 
     def send_results(src, dst, send, recv):
-        for d in range(NS):
+        for d in (3 - 3 * zh, 2 - zh, s1, s):
             @pl.when(jnp.logical_not(here(d)))
             def _():
                 result_copy(src, dst, send, recv, d).start()

time: 106 us -> 105 us (level)
  no operation moved by 1% of the time
where the time goes in v4:
time: 105 us
  Pallas kernels  104 us (99%)
    pallas_call x1, Pallas kernels, fused_device(): call(tokens, norm_gain.reshape(1, -1), ws, wq, wk, wv, dre, dim, logstep,...  103 us

profile of v4, /device:TPU:1, one launch (start us, length us, event | category | flops | bytes accessed | tf_op | source)
XLA Modules:
  0.0 105.0 jit_solution(10392442895012505057)
XLA Ops:
  0.6 102.6 %shard_map.194 = (bf16[1,64,4096]{2,1,0:T(8,128)(2,1)}, f32[1,4,2,128]{3,2,1,0:T(2,128)}) custom-call(bf16[1,128,2048]{2,1,0:T(8,128)(2,1)} %tok_ref.1, f32[1,4096]{1,0:T(1,128)} %bitcast.7, bf16[256,1024]{1,0:T(8,128)(2,1)} %ws_ref.1, bf16[256,1024]{1,0:T(8,128)(2,1)} %wq_ref.1, bf16[256,1024]{1,0:T(8,128)(2,1)} %wk_ref.1, bf16[256,1024]{1,0:T(8,128)(2,1)} %wv_ref.1, ...), custom_call_target="tpu_custom_call" | custom-call | tf_op jit(solution)/shard_map/pallas_call | solution.py:980
  103.2 1.8 %shard_map.195 = (bf16[1,64,4096]{2,1,0:T(8,128)(2,1)}, f32[1,4,2,128]{3,2,1,0:T(2,128)}) custom-call(bf16[1,64,4096]{2,1,0:T(8,128)(2,1)} %get-tuple-element.4.mixed_ref, f32[1,4,2,128]{3,2,1,0:T(2,128)} %get-tuple-element.5.logs_ref), custom_call_target="tpu_custom_call" | custom-call | tf_op jit(solution)/shard_map/pallas_call | solution.py:985

commit v5 on v4

--- a/solution.py
+++ b/solution.py
@@ -909,7 +909,7 @@
     NS, NT, L, D, CW = sizes
     KW, KB, HC = (D // 2, ws.shape[0], CW // NS)
     SEQ, G = (NS * L, HC // 16)
-    tiles, pieces = (4, 2)
+    tiles, pieces = (2, 2)
     bf, f32 = (jnp.bfloat16, jnp.float32)
     V = pltpu.VMEM
     DMA = pltpu.SemaphoreType.DMA
@@ -990,14 +990,14 @@
         ),
         in_specs=[hbm, hbm],
         out_specs=(hbm, hbm),
-        scratch_shapes=[V(mixed.shape, bf), V(logs.shape, f32), DMA((5,)), DMA((5,))],
+        scratch_shapes=[V(mixed.shape, bf), V(logs.shape, f32), DMA((3,)), DMA((3,))],
     )(mixed, logs)
 
 
 def hand_over(mixed_ref, logs_ref, mixed_out, logs_out, mixed_buf, logs_buf, in_sem, out_sem):
-    rows = mixed_buf.shape[1] // 4
+    rows = mixed_buf.shape[1] // 2
     views = [
-        tuple(ref.at[:, pl.ds(i * rows, rows)] for ref in (mixed_ref, mixed_buf, mixed_out)) for i in range(4)
+        tuple(ref.at[:, pl.ds(i * rows, rows)] for ref in (mixed_ref, mixed_buf, mixed_out)) for i in range(2)
     ]
     views.append((logs_ref, logs_buf, logs_out))
     loads = [pltpu.make_async_copy(v[0], v[1], in_sem.at[i]) for i, v in enumerate(views)]

time: 105 us -> 105 us (level)
  no operation moved by 1% of the time
where the time goes in v5:
time: 105 us
  Pallas kernels  104 us (99%)
    pallas_call x1, Pallas kernels, fused_device(): call(tokens, norm_gain.reshape(1, -1), ws, wq, wk, wv, dre, dim, logstep,...  102 us

profile of v5, /device:TPU:1, one launch (start us, length us, event | category | flops | bytes accessed | tf_op | source)
XLA Modules:
  0.0 104.9 jit_solution(1204553522654638498)
XLA Ops:
  0.6 102.5 %shard_map.194 = (bf16[1,64,4096]{2,1,0:T(8,128)(2,1)}, f32[1,4,2,128]{3,2,1,0:T(2,128)}) custom-call(bf16[1,128,2048]{2,1,0:T(8,128)(2,1)} %tok_ref.1, f32[1,4096]{1,0:T(1,128)} %bitcast.7, bf16[256,1024]{1,0:T(8,128)(2,1)} %ws_ref.1, bf16[256,1024]{1,0:T(8,128)(2,1)} %wq_ref.1, bf16[256,1024]{1,0:T(8,128)(2,1)} %wk_ref.1, bf16[256,1024]{1,0:T(8,128)(2,1)} %wv_ref.1, ...), custom_call_target="tpu_custom_call" | custom-call | tf_op jit(solution)/shard_map/pallas_call | solution.py:980
  103.1 1.8 %shard_map.195 = (bf16[1,64,4096]{2,1,0:T(8,128)(2,1)}, f32[1,4,2,128]{3,2,1,0:T(2,128)}) custom-call(bf16[1,64,4096]{2,1,0:T(8,128)(2,1)} %get-tuple-element.4.mixed_ref, f32[1,4,2,128]{3,2,1,0:T(2,128)} %get-tuple-element.5.logs_ref), custom_call_target="tpu_custom_call" | custom-call | tf_op jit(solution)/shard_map/pallas_call | solution.py:985
